TPU v7x, 256 devices: a whole 4x4x8 slice. The times are simulated.
256 devices in a mesh: sp: 64 (over z, y, core), tp: 4 (over x).
Axes of the slice: x: 4, y: 4, z: 8, core: 2. Of those that a mesh axis runs over, the one named last changes fastest.
Arguments:
- tokens: bfloat16 [10240, 2048], P('sp'), may hold values from -6 to 6
- input_gain: float32 [2048], replicated, may hold values from 0.1 to 1.9
- chain_query: bfloat16 [2048, 1024], P('sp', 'tp'), may hold values from -0.125 to 0.125
- forward_gate: bfloat16 [2048, 1024], P('sp', 'tp'), may hold values from -0.125 to 0.125
- backward_gate: bfloat16 [2048, 1024], P('sp', 'tp'), may hold values from -0.125 to 0.125
- chain_value: bfloat16 [2048, 1024], P('sp', 'tp'), may hold values from -0.125 to 0.125
- output_gate: bfloat16 [2048, 1024], P('sp', 'tp'), may hold values from -0.125 to 0.125
- forget_rate: float32 [2, 1024], P(None, 'tp'), may hold values from 0.2 to 6
- chain_gain: float32 [1024], P('tp'), may hold values from 0.1 to 1.9
- query_down: bfloat16 [2048, 768], P('sp'), may hold values from -0.125 to 0.125
- latent_down: bfloat16 [2048, 512], P('sp'), may hold values from -0.125 to 0.125
- rotary_down: bfloat16 [2048, 64], replicated, may hold values from -0.125 to 0.125
- query_latent_gain: float32 [768], replicated, may hold values from 0.1 to 1.9
- latent_gain: float32 [512], replicated, may hold values from 0.1 to 1.9
- query_up: bfloat16 [768, 1536], P(None, 'tp'), may hold values from -0.21875 to 0.21875
- latent_up: bfloat16 [512, 2048], P(None, 'tp'), may hold values from -0.25 to 0.25
- query_head_gain: float32 [192], replicated, may hold values from 0.1 to 1.9
- key_head_gain: float32 [192], replicated, may hold values from 0.1 to 1.9
- mixer_gain: float32 [1024], P('tp'), may hold values from 0.1 to 1.9
- chain_out: bfloat16 [1024, 2048], P('tp', 'sp'), may hold values from -0.125 to 0.125
- attend_out: bfloat16 [1024, 2048], P('tp', 'sp'), may hold values from -0.125 to 0.125
Outputs:
- mixed: float32 [10240, 2048], P(('sp', 'tp'))
All inputs are finite; a program needn't handle non-finite values.
Results may differ from a plain program's by a relative error of at most 0.017.
Values may be sent and summed in bfloat16 or wider, within the bound.
No kernel may reach another device: no remote copies, remote signals or barrier semaphores. Data moves between devices by JAX's collectives and lax.ppermute only.
A program may use at most 128 MiB of HBM per device.

v0:
```python
import jax
import jax.numpy as jnp
from jax import lax
from jax.experimental import pallas as pl
from jax.experimental.pallas import tpu as pltpu
from jax.sharding import Mesh
from jax.sharding import PartitionSpec as P

HEAD = 128
ROPE = 64
QK = 192
QLAT = 768
KVLAT = 512
Q8 = QLAT // 8
KV8 = KVLAT // 8
NZ, NY, NC, NX = 8, 4, 2, 4
EPS = 1e-06
THETA = 10000.0
SP = ("z", "y", "c")
F32 = jnp.float32
BF = jnp.bfloat16
VMEM_GRANT = 20 << 20
LOG2E = 1.4426950408889634


def shift(value, axis, count, by):
    return lax.ppermute(value, axis, [(i, (i + by) % count) for i in range(count)])


def exchange(value, axis):
    return lax.all_to_all(value, axis, 0, 0, tiled=True)


def ring_z(piece):
    found = [piece]
    up = down = piece
    for k in range(1, NZ // 2 + 1):
        up = shift(up, "z", NZ, 1)
        found.append(up)
        if k < NZ // 2:
            down = shift(down, "z", NZ, -1)
            found.append(down)
    return found


def spread_y(piece):
    half = NZ // 2
    right = shift(piece, "y", NY, 1)
    left = shift(piece, "y", NY, -1)
    far = shift(right[:half], "y", NY, 1), shift(left[half:], "y", NY, -1)
    return [piece, right, left, *far]


def dot(a, b):
    return lax.dot_general(a, b, (((1,), (0,)), ((), ())), preferred_element_type=F32)


def dot_nt(a, b):
    return lax.dot_general(a, b, (((1,), (1,)), ((), ())), preferred_element_type=F32)


def dot_tn(a, b):
    return lax.dot_general(a, b, (((0,), (0,)), ((), ())), preferred_element_type=F32)


def inverse_rms(square_sum, width):
    return lax.rsqrt(square_sum * (1.0 / width) + EPS)


def squares(values):
    return jnp.sum(values * values, axis=-1, keepdims=True)


def call(body, outs, args, scratch=(), specs=None, flops=1 << 20, grid=()):
    whole = pl.BlockSpec(memory_space=pltpu.VMEM)
    single = not isinstance(outs, list)
    return pl.pallas_call(
        body,
        out_shape=outs,
        grid=grid,
        in_specs=[whole if specs is None or specs[i] is None else specs[i] for i in range(len(args))],
        out_specs=whole if single else [whole] * len(outs),
        scratch_shapes=list(scratch),
        cost_estimate=pl.CostEstimate(flops=flops, bytes_accessed=1 << 20, transcendentals=0),
        compiler_params=pltpu.CompilerParams(vmem_limit_bytes=VMEM_GRANT),
    )(*args)


def made(shape, dtype):
    return jax.ShapeDtypeStruct(shape, dtype)


def prep_low_kernel(qd, ld, out):
    x = lax.axis_index("x")
    n = qd.shape[0]
    half = n // 2
    for j in range(NC):
        out[0, j, n : n + half, :] = jnp.zeros((half, HEAD), BF)
        for i in range(NX):

            @pl.when(x == i)
            def _():
                e = i * NC + j
                out[0, j, 0:n, 0:64] = qd[:, e * Q8 : e * Q8 + 64]
                out[0, j, 0:n, 64:128] = ld[:, e * KV8 : (e + 1) * KV8]
                for g in range(2):
                    rows = slice(g * half, (g + 1) * half)
                    lanes = slice(32 * g, 32 * g + 32)
                    out[0, j, n : n + half, lanes] = qd[rows, e * Q8 + 64 : (e + 1) * Q8]

        ready = out[0, j, :, :]
        for k in range(1, NZ):
            out[k, j, :, :] = ready


def prep_kernel(after, cq, fg, bg, cv, og, co, ao, out):
    for j in range(NC):
        lanes = slice(j * HEAD, (j + 1) * HEAD)
        for k in range(NZ):
            for i, w in enumerate((cq, fg, bg, cv, og, co, ao)):
                out[k, j, :, i * HEAD : (i + 1) * HEAD] = w[:, lanes]


def ups_kernel(q_up, kv_up, q_gain, kv_gain, wq, wkv, gq, gkv):
    c, x = lax.axis_index("c"), lax.axis_index("x")
    for i in range(8):
        e = lax.rem(x - i // NC + NX, NX) * NC + (c if i % NC == 0 else 1 - c)
        row = pl.multiple_of(e * Q8, 32)
        for part, size, at in ((0, 64, i * 64), (64, 32, 512 + i * 32)):
            rows = q_up[pl.ds(row + part, size), :]
            wq[at : at + size, :] = jnp.where(c == 0, rows[:, 0:QK], rows[:, QK : 2 * QK])
            gq[:, at : at + size] = q_gain[pl.ds(e, 1), part : part + size]
        row = pl.multiple_of(e * KV8, 64)
        lanes = pl.ds(pl.multiple_of(c * 256, 256), 256)
        wkv[i * 64 : (i + 1) * 64, :] = kv_up[pl.ds(row, 64), lanes]
        gkv[:, i * 64 : (i + 1) * 64] = kv_gain[pl.ds(e, 1), :]


def gather_rows(scr, sems, refs, lanes):
    y = lax.axis_index("y")
    half = NZ // 2
    every = slice(0, NZ)
    copies = []
    if len(refs) == NY:
        plan = [(k, every) for k in range(NY)]
    else:
        plan = [(0, every), (1, every), (3, every), (2, slice(0, half)), (2, slice(half, NZ))]
    for i, (ref, (back, rows)) in enumerate(zip(refs, plan)):
        spot = scr.at[rows, lax.rem(y - back + NY, NY)]
        copies.append(pltpu.make_async_copy(ref.at[:, :, lanes], spot, sems.at[i]))
    for copy in copies:
        copy.start()
    return copies


def gathered(scr, copies):
    for copy in copies:
        copy.wait()
    return scr[...].reshape(-1, scr.shape[-1])


def low_kernel(mine, other, gain, rot, b0, b1, b2, b3, normed, low, rotary, p_scr, w_scr, sems):
    c = lax.axis_index("c")
    copies = gather_rows(p_scr, sems, (b0, b1, b2, b3), slice(0, HEAD))
    half = mine.shape[0]
    for ref, at in ((mine, c), (other, 1 - c)):

        def some(i, carry):
            values = ref[pl.ds(pl.multiple_of(i * 32, 32), 32), :].astype(F32)
            values = values * inverse_rms(squares(values), values.shape[1]) * gain[...]
            row = pl.multiple_of(at * half + i * 32, 32)
            normed[pl.ds(row, 32), :] = values.astype(BF)
            return carry

        lax.fori_loop(0, half // 32, some, 0)
    rotary[...] = dot_nt(normed[...], rot[...]).astype(BF)
    for copy in copies:
        copy.wait()
    size = w_scr.shape[0] // (NZ * NY * NC)
    for i in range(NZ):
        for j in range(NY):
            for k in range(NC):
                at = (i * NY * NC + j * NC + k) * size
                top = k * size * 3 // 2
                w_scr[at : at + size, 0:HEAD] = p_scr[i, j, top : top + size, :]
                rest = p_scr[i, j, top + size : top + size * 3 // 2, :]
                for g in range(2):
                    row = at + g * size // 2
                    w_scr[row : row + size // 2, HEAD : HEAD + 32] = rest[:, 32 * g : 32 * g + 32]
    ready = dot(normed[...], w_scr[...]).astype(BF)
    n = 2 * half
    low[0:n, :] = ready[:, 0:HEAD]
    for k in range(4):
        low[n : n + n // 4, 32 * k : 32 * k + 32] = ready[k * n // 4 : (k + 1) * n // 4, HEAD : HEAD + 32]


def chain_kernel(
    after,
    rates,
    normed,
    a0,
    a1,
    a2,
    a3,
    a4,
    inside,
    probe_f,
    probe_b,
    packet,
    w_scr,
    sems,
):
    copies = gather_rows(w_scr, sems, (a0, a1, a2, a3, a4), slice(0, 512))
    acc = dot(normed[...], gathered(w_scr, copies))
    ready = acc.astype(BF)
    n = ready.shape[0]
    query = ready[:, 0:128].astype(F32)
    payload = ready[:, 384:512]
    row = lax.broadcasted_iota(jnp.int32, (n, n), 0)
    col = lax.broadcasted_iota(jnp.int32, (n, n), 1)
    within = None
    logs = []
    for d in range(2):
        keep = (row >= col) if d == 0 else (row <= col)
        logit = ready[:, 128 * (d + 1) : 128 * (d + 2)].astype(F32)
        key = rates[d : d + 1, :] * jax.nn.sigmoid(-logit)
        log = jnp.log1p(-key)
        high = log.astype(BF)
        rest = (log - high.astype(F32)).astype(BF)
        tri = keep.astype(BF)
        cum = dot(tri, high) + dot(tri, rest)
        total = cum[n - 1 : n, :] if d == 0 else cum[0:1, :]
        probe = (query * jnp.exp(cum)).astype(BF)
        look = (key * jnp.exp(-cum)).astype(BF)
        (probe_f if d == 0 else probe_b)[...] = probe
        score = jnp.where(keep, dot_nt(probe, look), 0.0)
        within = score if within is None else within + score
        digest = dot_tn(payload, (key * jnp.exp(total - cum)).astype(BF)).astype(BF)
        for k in range(NY):
            packet[k, d * HEAD : (d + 1) * HEAD, :] = digest
        high = total.astype(BF).astype(F32)
        logs += [high, total - high]
    inside[...] = dot(within.astype(BF), payload)
    at = lax.broadcasted_iota(jnp.int32, (16, HEAD), 0)
    tail = jnp.zeros((16, HEAD), F32)
    for i, log in enumerate(logs):
        tail = jnp.where(at == i, log, tail)
    for k in range(NY):
        packet[k, 2 * HEAD : 2 * HEAD + 16, :] = tail.astype(BF)


def walk(states, logs, order, chosen):
    state = jnp.zeros((HEAD, HEAD), F32)
    log = jnp.zeros((1, HEAD), F32)
    for j in order:
        fresh = state * jnp.exp(logs(j)) + states(j)
        passed = chosen(j)
        state = jnp.where(passed, fresh, state)
        log = jnp.where(passed, log + logs(j), log)
    return state, log


def slab_kernel(slab, state_f, state_b, log_out, send):
    z, y = lax.axis_index("z"), lax.axis_index("y")
    at = lax.broadcasted_iota(jnp.int32, (16, HEAD), 0)
    kept = []
    for d in range(2):
        order = range(NY) if d == 0 else range(NY - 1, -1, -1)

        def states(j):
            return slab[j, d * HEAD : (d + 1) * HEAD, :].astype(F32)

        def logs(j):
            block = slab[j, 2 * HEAD : 2 * HEAD + 16, :].astype(F32)
            return block[2 * d : 2 * d + 1, :] + block[2 * d + 1 : 2 * d + 2, :]

        part, log = walk(states, logs, order, (lambda j: j < y) if d == 0 else (lambda j: j > y))
        full, full_log = walk(states, logs, order, lambda j: j >= 0)
        (state_f if d == 0 else state_b)[...] = part
        log_out[d : d + 1, :] = log
        high = full_log.astype(BF).astype(F32)
        tail = jnp.where(at == 0, high, jnp.where(at == 1, full_log - high, 0.0)).astype(BF)
        kept.append((full.astype(BF), tail))
    for k in range(NZ):
        ahead = k > z
        send[k, 0:HEAD, :] = jnp.where(ahead, kept[0][0], kept[1][0])
        send[k, HEAD : HEAD + 16, :] = jnp.where(ahead, kept[0][1], kept[1][1])


def close_kernel(
    outer,
    state_f,
    state_b,
    log_in,
    probe_f,
    probe_b,
    inside,
    gain,
    normed,
    l0,
    l1,
    l2,
    l3,
    mixed,
    w_scr,
    sems,
):
    copies = gather_rows(w_scr, sems, (l0, l1, l2, l3), slice(0, HEAD))
    z = lax.axis_index("z")
    combined = inside[...]
    for d in range(2):
        order = range(NZ) if d == 0 else range(NZ - 1, -1, -1)

        def states(j):
            return outer[j, 0:HEAD, :].astype(F32)

        def logs(j):
            block = outer[j, HEAD : HEAD + 16, :].astype(F32)
            return block[0:1, :] + block[1:2, :]

        far, _ = walk(states, logs, order, (lambda j: j < z) if d == 0 else (lambda j: j > z))
        near = (state_f if d == 0 else state_b)[...]
        state = near + far * jnp.exp(log_in[d : d + 1, :])
        probe = (probe_f if d == 0 else probe_b)[...]
        combined = combined + dot_nt(probe, state.astype(BF))
    opened = dot(normed[...], gathered(w_scr, copies)).astype(BF).astype(F32)
    opened = opened * jax.nn.sigmoid(opened)
    scale = inverse_rms(squares(combined), HEAD)
    mixed[...] = (combined * scale * gain[...] * opened).astype(BF)


def heads_kernel(*refs):
    swapped, wq, wkv, gq, gkv, rotary, cos, sin, qh_gain, kh_gain = refs[4:14]
    q_out, kv_out, q_scr, kv_scr = refs[14:]
    n = rotary.shape[0]
    half = n // 2
    size = n + n // 4
    for i in range(2 * NX):
        ref = refs[i // 2] if i % 2 == 0 else swapped.at[i // 2 * size : (i // 2 + 1) * size]
        q_scr[:, i * 64 : (i + 1) * 64] = ref[0:n, 0:64]
        kv_scr[:, i * 64 : (i + 1) * 64] = ref[0:n, 64:128]
        for k in range(4):
            rows = slice(k * n // 4, (k + 1) * n // 4)
            q_scr[rows, 512 + 32 * i : 544 + 32 * i] = ref[n : n + n // 4, 32 * k : 32 * k + 32]

    def latent(scr, width, up, gain):
        values = scr[...].astype(F32)
        values = values * inverse_rms(squares(values), width) * gain[...]
        return dot(values.astype(BF), up[...]).astype(BF)

    query = latent(q_scr, QLAT, wq, gq).astype(F32)
    pairs = latent(kv_scr, KVLAT, wkv, gkv)

    def turned(tail):
        swapped = jnp.concatenate([tail[:, ROPE // 2 :], tail[:, : ROPE // 2]], axis=1)
        return (tail * cos[...] + swapped * sin[...]).astype(BF)

    scale = inverse_rms(squares(query), QK)
    query = query * scale * qh_gain[...]
    nope = query[:, 0:HEAD].astype(BF)
    tail = turned(query[:, HEAD:QK])
    for k in range(NY):
        q_out[k, 0:n, :] = nope
        q_out[k, n : n + half, 0:ROPE] = tail[0:half]
        q_out[k, n : n + half, ROPE:HEAD] = tail[half:n]
    key = pairs[:, 0:HEAD].astype(F32)
    rope = rotary[...].astype(F32)
    scale = inverse_rms(squares(key) + squares(rope), QK)
    kv_out[0:n, :] = (key * scale * kh_gain[:, 0:HEAD]).astype(BF)
    kv_out[n : 2 * n, :] = pairs[:, HEAD : 2 * HEAD]
    tail = turned(rope * scale * kh_gain[:, HEAD:QK])
    kv_out[2 * n : 2 * n + half, 0:ROPE] = tail[0:half]
    kv_out[2 * n : 2 * n + half, ROPE:HEAD] = tail[half:n]


def attend_kernel(*refs):
    queries, kv_refs = refs[0], refs[1 : 1 + NZ]
    outs = refs[1 + NZ : 1 + NZ + NY]
    q_scr, key_scr, val_scr = refs[1 + NZ + NY :]
    y = lax.axis_index("y")
    n = queries.shape[1] * 2 // 3
    half = n // 2
    for i, kv in enumerate(kv_refs):
        at = i * n
        key_scr[at : at + n, 0:HEAD] = kv[0:n, :]
        tail = kv[2 * n : 2 * n + half, :]
        key_scr[at : at + half, HEAD:QK] = tail[:, 0:ROPE]
        key_scr[at + half : at + n, HEAD:QK] = tail[:, ROPE:HEAD]
        val_scr[at : at + n, 0:HEAD] = kv[n : 2 * n, :]
    val_scr[:, HEAD : 2 * HEAD] = jnp.ones((NZ * n, HEAD), BF)
    diagonal = lax.broadcasted_iota(jnp.int32, (HEAD, HEAD), 0) == lax.broadcasted_iota(
        jnp.int32, (HEAD, HEAD), 1
    )
    row = lax.broadcasted_iota(jnp.int32, (16, HEAD), 0)
    for k, out in enumerate(outs):
        at = lax.rem(y + k, NY)
        q_scr[0:n, 0:HEAD] = queries[at, 0:n, :]
        tail = queries[at, n : n + half, :]
        q_scr[0:half, HEAD:QK] = tail[:, 0:ROPE]
        q_scr[half:n, HEAD:QK] = tail[:, ROPE:HEAD]
        scores = dot_nt(q_scr[...], key_scr[...])
        weights = jnp.exp2(scores * (QK**-0.5 * LOG2E)).astype(BF)
        sums = dot(weights, val_scr[...])
        out[0:n, :] = sums[:, 0:HEAD].astype(BF)
        tail = jnp.zeros((16, HEAD), F32)
        for b in range(0, n, HEAD):
            size = min(HEAD, n - b)
            den = sums[b : b + size, HEAD : 2 * HEAD]
            line = jnp.sum(jnp.where(diagonal[0:size], den, 0.0), axis=0, keepdims=True)
            high = line.astype(BF).astype(F32)
            tail = jnp.where(row == 2 * (b // HEAD), high, tail)
            tail = jnp.where(row == 2 * (b // HEAD) + 1, line - high, tail)
        out[n : n + 16, :] = tail.astype(BF)


def attend(queries, pieces):
    n = pieces[0].shape[0] * 2 // 5
    return call(
        attend_kernel,
        [made((n + 16, HEAD), BF)] * NY,
        [queries] + list(pieces),
        scratch=[
            pltpu.VMEM((n, QK), BF),
            pltpu.VMEM((NZ * n, QK), BF),
            pltpu.VMEM((NZ * n, 2 * HEAD), BF),
        ],
        flops=2 * NY * n * NZ * n * 512,
    )


def final_kernel(
    p0, p1, p2, p3, chain, gain, o0, o1, o2, o3, mine, theirs, scr, w_scr, sems
):
    c, x = lax.axis_index("c"), lax.axis_index("x")
    n = chain.shape[0]
    half = n // 2
    quarter = half // NX
    parts = (p0, p1, p2, p3)
    copies = gather_rows(w_scr, sems, (o0, o1, o2, o3), slice(HEAD, 3 * HEAD))
    sums = lines = None
    for part in parts:
        values = part[0:n, :].astype(F32)
        line = part[n : n + 16, :].astype(F32)
        sums = values if sums is None else sums + values
        lines = line if lines is None else lines + line
    row = lax.broadcasted_iota(jnp.int32, (HEAD, HEAD), 0)
    diagonal = row == lax.broadcasted_iota(jnp.int32, (HEAD, HEAD), 1)
    scr[:, 0:HEAD] = chain[...].astype(F32)
    for b in range(0, n, HEAD):
        size = min(HEAD, n - b)
        i = 2 * (b // HEAD)
        line = lines[i : i + 1, :] + lines[i + 1 : i + 2, :]
        den = jnp.sum(jnp.where(diagonal, line, 0.0), axis=1, keepdims=True)[0:size]
        rows = sums[b : b + size] / den
        scale = inverse_rms(squares(rows), HEAD)
        scr[b : b + size, HEAD : 2 * HEAD] = rows * scale * gain[...]
    weight = gathered(w_scr, copies)
    for out, core in ((mine, c), (theirs, 1 - c)):
        picked = []
        for k in range(NX):
            at = core * half + lax.rem(x + k, NX) * quarter
            picked.append(scr[pl.ds(pl.multiple_of(at, 8), quarter), :])
        mixed = jnp.concatenate(picked, axis=0).astype(BF)
        out[...] = dot_nt(mixed, weight).astype(out.dtype)


def on_device(
    tokens,
    input_gain,
    chain_query,
    forward_gate,
    backward_gate,
    chain_value,
    output_gate,
    forget_rate,
    chain_gain,
    query_down,
    latent_down,
    rotary_down,
    query_latent_gain,
    latent_gain,
    query_up,
    latent_up,
    query_head_gain,
    key_head_gain,
    mixer_gain,
    chain_out,
    attend_out,
):
    z, y, c, _ = (lax.axis_index(a) for a in ("z", "y", "c", "x"))
    rows, width = tokens.shape
    n = rows * NC
    seq_len = n * NY * NZ
    piece = chain_query.shape[0]

    def cols(weight, size):
        return lax.dynamic_slice_in_dim(weight, c * size, size, 1)

    send_b = call(
        prep_low_kernel, made((NZ, NC, piece * 3 // 2, HEAD), BF), (query_down, latent_down)
    )
    anywhere = pl.BlockSpec(memory_space=pl.ANY)
    send_a = call(
        prep_kernel,
        made((NZ, NC, piece, 896), BF),
        (
            send_b,
            chain_query,
            forward_gate,
            backward_gate,
            chain_value,
            output_gate,
            chain_out.T,
            attend_out.T,
        ),
        specs=[anywhere] + [None] * 7,
    )

    def along_z(value):
        flat = value.reshape((NZ * NC,) + value.shape[2:])
        return exchange(flat, ("z", "c")).reshape(NZ, -1, value.shape[-1])

    other = shift(tokens, "c", NC, 1)
    column_b = along_z(send_b)
    column_a = along_z(send_a)
    column_a, column_l = column_a[:, :, :512], column_a[:, :, 512:]
    weights_b = [column_b] + [shift(column_b, "y", NY, k) for k in range(1, NY)]
    weights_a = spread_y(column_a)
    weights_l = [column_l] + [shift(column_l, "y", NY, k) for k in range(1, NY)]

    positions = ((z * NY + y) * n + jnp.arange(n, dtype=jnp.int32)).astype(F32)
    inverse = THETA ** (-jnp.arange(0, ROPE, 2).astype(F32) / ROPE)
    angles = positions[:, None] * inverse
    cosine, sine = jnp.cos(angles), jnp.sin(angles)
    early = [
        jnp.concatenate([cosine, cosine], axis=1),
        jnp.concatenate([-sine, sine], axis=1),
        cols(forget_rate, HEAD) / seq_len,
        lax.dynamic_slice_in_dim(chain_gain[None], c * HEAD, HEAD, 1),
        lax.dynamic_slice_in_dim(mixer_gain[None], c * HEAD, HEAD, 1),
    ]
    early += call(
        ups_kernel,
        [
            made((QLAT, QK), BF),
            made((KVLAT, 2 * HEAD), BF),
            made((1, QLAT), F32),
            made((1, KVLAT), F32),
        ],
        (query_up, latent_up, query_latent_gain.reshape(8, Q8), latent_gain.reshape(8, KV8)),
    )
    weights_b[3], early = lax.optimization_barrier((weights_b[3], early))
    cos2, sin2, rates, gain_c, gain_m, wq, wkv, gq, gkv = early
    normed, low, rotary = call(
        low_kernel,
        [made((n, width), BF), made((n * 5 // 4, HEAD), BF), made((n, ROPE), BF)],
        [tokens, other, input_gain[None], rotary_down.T] + weights_b,
        scratch=[
            pltpu.VMEM((NZ, NY, NC * piece * 3 // 2, HEAD), BF),
            pltpu.VMEM((width, HEAD + 32), BF),
            pltpu.SemaphoreType.DMA((4,)),
        ],
        specs=[None] * 4 + [anywhere] * 4,
        flops=2 * n * width * 320,
    )
    pieces = [low] + [shift(low, "x", NX, k) for k in range(1, NX)]
    swapped = shift(jnp.concatenate(pieces, axis=0), "c", NC, 1)
    queries, kv_piece = call(
        heads_kernel,
        [made((NY, n * 3 // 2, HEAD), BF), made((n * 5 // 2, HEAD), BF)],
        pieces
        + [swapped, wq, wkv, gq, gkv, rotary, cos2, sin2, query_head_gain[None], key_head_gain[None]],
        scratch=[pltpu.VMEM((n, QLAT), BF), pltpu.VMEM((n, KVLAT), BF)],
        flops=2 * n * (QLAT * QK + KVLAT * 256),
    )
    kv = ring_z(kv_piece)
    all_queries = exchange(queries, "y")
    part = attend(all_queries, kv)
    parts = [part[0]] + [shift(part[k], "y", NY, k) for k in range(1, NY)]

    inside, probe_f, probe_b, packet = call(
        chain_kernel,
        [
            made((n, HEAD), F32),
            made((n, HEAD), BF),
            made((n, HEAD), BF),
            made((NY, 2 * HEAD + 16, HEAD), BF),
        ],
        [all_queries, rates, normed] + weights_a,
        scratch=[pltpu.VMEM((NZ, NY, NC * piece, 512), BF), pltpu.SemaphoreType.DMA((5,))],
        specs=[anywhere, None, None] + [anywhere] * 5,
        flops=2 * n * width * 512,
    )
    slab = exchange(packet, "y")
    state_f, state_b, log_in, send = call(
        slab_kernel,
        [
            made((HEAD, HEAD), F32),
            made((HEAD, HEAD), F32),
            made((2, HEAD), F32),
            made((NZ, HEAD + 16, HEAD), BF),
        ],
        (slab,),
    )
    outer = exchange(send, "z")

    chain_mixed = call(
        close_kernel,
        made((n, HEAD), BF),
        (
            outer,
            state_f,
            state_b,
            log_in,
            probe_f,
            probe_b,
            inside,
            gain_c,
            normed,
            *weights_l,
        ),
        scratch=[pltpu.VMEM((NZ, NY, NC * piece, HEAD), BF), pltpu.SemaphoreType.DMA((4,))],
        specs=[None] * 9 + [anywhere] * 4,
    )
    mine, theirs = call(
        final_kernel,
        [made((rows, width), F32), made((rows, width), BF)],
        parts + [chain_mixed, gain_m] + weights_l,
        scratch=[
            pltpu.VMEM((n, 2 * HEAD), F32),
            pltpu.VMEM((NZ, NY, NC * piece, 256), BF),
            pltpu.SemaphoreType.DMA((4,)),
        ],
        specs=[None] * 6 + [anywhere] * 4,
        flops=2 * n * width * 256,
    )
    summed = mine + shift(theirs, "c", NC, 1).astype(F32)
    quarter = rows // NX
    result = summed[:quarter]
    for k in range(1, NX):
        row = summed[k * quarter : (k + 1) * quarter].astype(BF)
        result = result + shift(row, "x", NX, k).astype(F32)
    return result


def solution(mesh):
    torus = Mesh(mesh.devices.reshape(NZ, NY, NC, NX), ("z", "y", "c", "x"))
    placed = (
        P(SP, None),
        P(),
        P(SP, "x"),
        P(SP, "x"),
        P(SP, "x"),
        P(SP, "x"),
        P(SP, "x"),
        P(None, "x"),
        P("x"),
        P(SP, None),
        P(SP, None),
        P(),
        P(),
        P(),
        P(None, "x"),
        P(None, "x"),
        P(),
        P(),
        P("x"),
        P("x", SP),
        P("x", SP),
    )

    return jax.shard_map(
        on_device, mesh=torus, in_specs=placed, out_specs=P(SP + ("x",), None), check_vma=False
    )
```

profile of v0, /device:TPU:1, one launch (start us, length us, event | category | flops | bytes accessed | tf_op | source)
XLA Modules:
  0.0 156.1 jit_solution(15385833826883478998)
XLA Ops:
  2.4 10.0 %all-to-all-start = ((bf16[16,48,128]{2,1,0:T(8,128)(2,1)}), bf16[16,48,128]{2,1,0:T(8,128)(2,1)S(1)}, u32[]{:S(2)}, u32[]{:S(2)}) async-start(bf16[16,48,128]{2,1,0:T(8,128)(2,1)} %bitcast.2), calls=%async_computation | async-start | bytes 393216 | tf_op jit(solution)/shard_map/all_to_all | solution.py:31
  18.5 4.1 %all-to-all-done = bf16[16,48,128]{2,1,0:T(8,128)(2,1)S(1)} async-done(((bf16[16,48,128]{2,1,0:T(8,128)(2,1)}), bf16[16,48,128]{2,1,0:T(8,128)(2,1)S(1)}, u32[]{:S(2)}, u32[]{:S(2)}) %all-to-all-start) | async-done | bytes 196640 | tf_op jit(solution)/shard_map/all_to_all | solution.py:31
  22.6 4.3 %all-to-all-start.2 = ((bf16[16,32,896]{2,1,0:T(8,128)(2,1)}), bf16[16,32,896]{2,1,0:T(8,128)(2,1)}, u32[]{:S(2)}, u32[]{:S(2)}) async-start(bf16[16,32,896]{2,1,0:T(8,128)(2,1)} %bitcast.10), calls=%async_computation.2 | async-start | bytes 1835008 | tf_op jit(solution)/shard_map/all_to_all | solution.py:31
  28.3 2.8 %collective-permute-start.3 = (bf16[8,96,128]{2,1,0:T(8,128)(2,1)S(1)}, bf16[8,96,128]{2,1,0:T(8,128)(2,1)S(1)}, u32[]{:S(2)}, u32[]{:S(2)}) collective-permute-start(bf16[8,96,128]{2,1,0:T(8,128)(2,1)S(1)} %bitcast.14), channel_id=1, source_target_pairs={{0,24},{8,0},{16,8},{24,16},{1,25},{9,1},{17,9},{25,17},{2,26},{10... | collective-permute-start | bytes 589832 | tf_op jit(solution)/shard_map/ppermute | solution.py:27
  34.8 4.3 %collective-permute-done.1.b1 = bf16[8,96,128]{2,1,0:T(8,128)(2,1)S(1)} collective-permute-done((bf16[8,96,128]{2,1,0:T(8,128)(2,1)S(1)}, bf16[8,96,128]{2,1,0:T(8,128)(2,1)S(1)}, u32[]{:S(2)}, u32[]{:S(2)}) %collective-permute-start.1) | collective-permute-done | bytes 196640 | tf_op jit(solution)/shard_map/ppermute | solution.py:27
  39.1 2.2 %collective-permute-done.2.b2 = bf16[8,96,128]{2,1,0:T(8,128)(2,1)S(1)} collective-permute-done((bf16[8,96,128]{2,1,0:T(8,128)(2,1)S(1)}, bf16[8,96,128]{2,1,0:T(8,128)(2,1)S(1)}, u32[]{:S(2)}, u32[]{:S(2)}) %collective-permute-start.2) | collective-permute-done | bytes 196640 | tf_op jit(solution)/shard_map/ppermute | solution.py:27
  41.4 3.3 %shard_map.201 = (bf16[320,2048]{1,0:T(8,128)(2,1)S(1)}, bf16[400,128]{1,0:T(8,128)(2,1)S(1)}, bf16[320,64]{1,0:T(8,128)(2,1)S(1)}) custom-call(bf16[160,2048]{1,0:T(8,128)(2,1)S(1)} %copy-done, bf16[160,2048]{1,0:T(8,128)(2,1)S(1)} %collective-permute-done.other, f32[1,2048]{1,0:T(1,128)S(1)} %bitcast.21, bf16[64,2048]{1,0:T(8,128)(2,1)S(1)} %bitcast.18, ...), custom_call_target="tpu_custom_call" | custom-call | flops 419430400 | bytes 1048576 | tf_op jit(solution)/shard_map/pallas_call | solution.py:77
  46.0 2.5 %collective-permute-start.5 = (bf16[400,128]{1,0:T(8,128)(2,1)S(1)}, bf16[400,128]{1,0:T(8,128)(2,1)S(1)}, u32[]{:S(2)}, u32[]{:S(2)}) collective-permute-start(bf16[400,128]{1,0:T(8,128)(2,1)S(1)} %get-tuple-element.43.refs_0_), channel_id=1, source_target_pairs={{0,2},{1,3},{2,0},{3,1},{4,6},{5,7},{6,4},{7,5},{8,10},{9,11},{10,... | collective-permute-start | bytes 307208 | tf_op jit(solution)/shard_map/ppermute | solution.py:27
  49.7 2.0 %collective-permute-done.5.refs_2_ = bf16[400,128]{1,0:T(8,128)(2,1)S(1)} collective-permute-done((bf16[400,128]{1,0:T(8,128)(2,1)S(1)}, bf16[400,128]{1,0:T(8,128)(2,1)S(1)}, u32[]{:S(2)}, u32[]{:S(2)}) %collective-permute-start.5) | collective-permute-done | bytes 102432 | tf_op jit(solution)/shard_map/ppermute | solution.py:27
  53.7 3.9 %collective-permute-start.7 = (bf16[1600,128]{1,0:T(8,128)(2,1)}, bf16[1600,128]{1,0:T(8,128)(2,1)}, u32[]{:S(2)}, u32[]{:S(2)}) collective-permute-start(bf16[1600,128]{1,0:T(8,128)(2,1)} %pad_maximum_fusion), channel_id=1, source_target_pairs={{0,4},{4,0},{1,5},{5,1},{2,6},{6,2},{3,7},{7,3},{8,12},{12,8},{9,1... | collective-permute-start | bytes 1228808 | tf_op jit(solution)/shard_map/ppermute | solution.py:27
  58.8 2.7 %collective-permute-start.19 = (bf16[8,64,512]{2,1,0:T(8,128)(2,1)S(1)}, bf16[8,64,512]{2,1,0:T(8,128)(2,1)S(1)}, u32[]{:S(2)}, u32[]{:S(2)}) collective-permute-start(bf16[8,64,512]{2,1,0:T(8,128)(2,1)S(1)} %slice.35.a0), channel_id=1, source_target_pairs={{0,24},{8,0},{16,8},{24,16},{1,25},{9,1},{17,9},{25,17},{2,26},{10... | collective-permute-start | bytes 1572872 | tf_op jit(solution)/shard_map/ppermute | solution.py:27
  65.3 3.3 %shard_map.202 = (bf16[4,480,128]{2,1,0:T(8,128)(2,1)S(1)}, bf16[800,128]{1,0:T(8,128)(2,1)}) custom-call(bf16[400,128]{1,0:T(8,128)(2,1)S(1)} %copy-done.6, bf16[400,128]{1,0:T(8,128)(2,1)S(1)} %collective-permute-done.4.refs_1_, bf16[400,128]{1,0:T(8,128)(2,1)S(1)} %collective-permute-done.5.refs_2_, bf16[400,128]{1,0:T(8,128)(2,1)S(1)} %collective-permute-done.6.refs_3_, ...), custom_call_target="tpu_custom_call" | custom-call | flops 178257920 | bytes 1048576 | tf_op jit(solution)/shard_map/pallas_call | solution.py:77
  69.9 3.5 %all-to-all-start.1 = ((bf16[4,480,128]{2,1,0:T(8,128)(2,1)}), bf16[4,480,128]{2,1,0:T(8,128)(2,1)S(1)}, u32[]{:S(2)}, u32[]{:S(2)}) async-start(bf16[4,480,128]{2,1,0:T(8,128)(2,1)} %copy-done.4), calls=%async_computation.1 | async-start | bytes 983040 | tf_op jit(solution)/shard_map/all_to_all | solution.py:31
  77.6 2.6 %collective-permute-start.9 = (bf16[800,128]{1,0:T(8,128)(2,1)}, bf16[800,128]{1,0:T(8,128)(2,1)}, u32[]{:S(2)}, u32[]{:S(2)}) collective-permute-start(bf16[800,128]{1,0:T(8,128)(2,1)} %get-tuple-element.52.refs_1_), channel_id=1, source_target_pairs={{0,224},{32,0},{64,32},{96,64},{128,96},{160,128},{192,160},{224,1... | collective-permute-start | bytes 614408 | tf_op jit(solution)/shard_map/ppermute | solution.py:27
  80.3 3.3 %collective-permute-done.9.refs_3_ = bf16[800,128]{1,0:T(8,128)(2,1)} collective-permute-done((bf16[800,128]{1,0:T(8,128)(2,1)}, bf16[800,128]{1,0:T(8,128)(2,1)}, u32[]{:S(2)}, u32[]{:S(2)}) %collective-permute-start.9) | collective-permute-done | bytes 204832 | tf_op jit(solution)/shard_map/ppermute | solution.py:27
  83.6 3.4 %collective-permute-start.11 = (bf16[800,128]{1,0:T(8,128)(2,1)}, bf16[800,128]{1,0:T(8,128)(2,1)}, u32[]{:S(2)}, u32[]{:S(2)}) collective-permute-start(bf16[800,128]{1,0:T(8,128)(2,1)} %collective-permute-done.9.refs_3_), channel_id=1, source_target_pairs={{0,224},{32,0},{64,32},{96,64},{128,96},{160,128},{192,160},{224,1... | collective-permute-start | bytes 614408 | tf_op jit(solution)/shard_map/ppermute | solution.py:27
  87.2 3.1 %shard_map.205 = (f32[320,128]{1,0:T(8,128)S(1)}, bf16[320,128]{1,0:T(8,128)(2,1)S(1)}, bf16[320,128]{1,0:T(8,128)(2,1)S(1)}, bf16[4,272,128]{2,1,0:T(8,128)(2,1)S(1)}) custom-call(bf16[4,480,128]{2,1,0:T(8,128)(2,1)S(1)} %all-to-all-done.1.refs_0_.after, f32[2,128]{1,0:T(2,128)S(1)} %dynamic-slice_multiply_fusion.rates, ...), custom_call_target="tpu_custom_call" | custom-call | flops 671088640 | bytes 1048576 | tf_op jit(solution)/shard_map/pallas_call | solution.py:77
  92.9 3.5 %all-to-all-start.3 = ((bf16[4,272,128]{2,1,0:T(8,128)(2,1)}), bf16[4,272,128]{2,1,0:T(8,128)(2,1)S(1)}, u32[]{:S(2)}, u32[]{:S(2)}) async-start(bf16[4,272,128]{2,1,0:T(8,128)(2,1)} %copy-done.9), calls=%async_computation.3 | async-start | bytes 557056 | tf_op jit(solution)/shard_map/all_to_all | solution.py:31
  96.4 2.6 %collective-permute-start.13 = (bf16[800,128]{1,0:T(8,128)(2,1)}, bf16[800,128]{1,0:T(8,128)(2,1)}, u32[]{:S(2)}, u32[]{:S(2)}) collective-permute-start(bf16[800,128]{1,0:T(8,128)(2,1)} %collective-permute-done.11.refs_5_), channel_id=1, source_target_pairs={{0,224},{32,0},{64,32},{96,64},{128,96},{160,128},{192,160},{224,1... | collective-permute-start | bytes 614408 | tf_op jit(solution)/shard_map/ppermute | solution.py:27
  99.0 2.9 %all-to-all-done.3.slab = bf16[4,272,128]{2,1,0:T(8,128)(2,1)S(1)} async-done(((bf16[4,272,128]{2,1,0:T(8,128)(2,1)}), bf16[4,272,128]{2,1,0:T(8,128)(2,1)S(1)}, u32[]{:S(2)}, u32[]{:S(2)}) %all-to-all-start.3) | async-done | bytes 278560 | tf_op jit(solution)/shard_map/all_to_all | solution.py:31
  103.4 6.3 %all-to-all-start.4 = ((bf16[8,144,128]{2,1,0:T(8,128)(2,1)}), bf16[8,144,128]{2,1,0:T(8,128)(2,1)}, u32[]{:S(2)}, u32[]{:S(2)}) async-start(bf16[8,144,128]{2,1,0:T(8,128)(2,1)} %get-tuple-element.60), calls=%async_computation.4 | async-start | bytes 589824 | tf_op jit(solution)/shard_map/all_to_all | solution.py:31
  111.1 1.9 %collective-permute-start.23 = (bf16[8,64,384]{2,1,0:T(8,128)(2,1)S(1)}, bf16[8,64,384]{2,1,0:T(8,128)(2,1)S(1)}, u32[]{:S(2)}, u32[]{:S(2)}) collective-permute-start(bf16[8,64,384]{2,1,0:T(8,128)(2,1)S(1)} %slice.38.l0.o0), channel_id=1, source_target_pairs={{0,16},{8,24},{16,0},{24,8},{1,17},{9,25},{17,1},{25,9},{2,18},{10... | collective-permute-start | bytes 1179656 | tf_op jit(solution)/shard_map/ppermute | solution.py:27
  113.6 6.0 %shard_map.203 = (bf16[336,128]{1,0:T(8,128)(2,1)S(1)}, bf16[336,128]{1,0:T(8,128)(2,1)}, bf16[336,128]{1,0:T(8,128)(2,1)}, bf16[336,128]{1,0:T(8,128)(2,1)}) custom-call(bf16[4,480,128]{2,1,0:T(8,128)(2,1)S(1)} %all-to-all-done.1.refs_0_.after, bf16[800,128]{1,0:T(8,128)(2,1)} %get-tuple-element.52.refs_1_, ...), custom_call_target="tpu_custom_call" | custom-call | flops 3355443200 | bytes 1048576 | tf_op jit(solution)/shard_map/pallas_call | solution.py:77
  122.6 2.1 %collective-permute-start.17 = (bf16[336,128]{1,0:T(8,128)(2,1)}, bf16[336,128]{1,0:T(8,128)(2,1)S(1)}, u32[]{:S(2)}, u32[]{:S(2)}) collective-permute-start(bf16[336,128]{1,0:T(8,128)(2,1)} %get-tuple-element.56), channel_id=1, source_target_pairs={{0,24},{8,0},{16,8},{24,16},{1,25},{9,1},{17,9},{25,17},{2,26},{10... | collective-permute-start | bytes 258056 | tf_op jit(solution)/shard_map/ppermute | solution.py:27
  124.6 2.8 %collective-permute-done.23.l2.o2 = bf16[8,64,384]{2,1,0:T(8,128)(2,1)S(1)} collective-permute-done((bf16[8,64,384]{2,1,0:T(8,128)(2,1)S(1)}, bf16[8,64,384]{2,1,0:T(8,128)(2,1)S(1)}, u32[]{:S(2)}, u32[]{:S(2)}) %collective-permute-start.23) | collective-permute-done | bytes 393248 | tf_op jit(solution)/shard_map/ppermute | solution.py:27
  127.4 4.2 %collective-permute-done.24.l3.o3 = bf16[8,64,384]{2,1,0:T(8,128)(2,1)S(1)} collective-permute-done((bf16[8,64,384]{2,1,0:T(8,128)(2,1)S(1)}, bf16[8,64,384]{2,1,0:T(8,128)(2,1)S(1)}, u32[]{:S(2)}, u32[]{:S(2)}) %collective-permute-start.24) | collective-permute-done | bytes 393248 | tf_op jit(solution)/shard_map/ppermute | solution.py:27
  136.0 2.0 %shard_map.207.chain = bf16[320,128]{1,0:T(8,128)(2,1)S(1)} custom-call(bf16[8,144,128]{2,1,0:T(8,128)(2,1)} %all-to-all-done.4.outer, f32[128,128]{1,0:T(8,128)S(1)} %copy-done.24, f32[128,128]{1,0:T(8,128)S(1)} %copy-done.26, f32[2,128]{1,0:T(2,128)S(1)} %get-tuple-element.63.log_in, bf16[320,128]{1,0:T(8,128)(2,1)S(1)} %copy-done.20, ...), custom_call_target="tpu_custom_call" | custom-call | flops 1048576 | bytes 1048576 | tf_op jit(solution)/shard_map/pallas_call | solution.py:77
  139.3 2.9 %collective-permute-start.25 = (bf16[160,2048]{1,0:T(8,128)(2,1)S(1)}, bf16[160,2048]{1,0:T(8,128)(2,1)S(1)}, u32[]{:S(2)}, u32[]{:S(2)}) collective-permute-start(bf16[160,2048]{1,0:T(8,128)(2,1)S(1)} %get-tuple-element.70), channel_id=1, source_target_pairs={{0,4},{4,0},{1,5},{5,1},{2,6},{6,2},{3,7},{7,3},{8,12},{12,8},{9,1... | collective-permute-start | bytes 1966088 | tf_op jit(solution)/shard_map/ppermute | solution.py:27
  142.2 1.7 %collective-permute-done.25 = bf16[160,2048]{1,0:T(8,128)(2,1)S(1)} collective-permute-done((bf16[160,2048]{1,0:T(8,128)(2,1)S(1)}, bf16[160,2048]{1,0:T(8,128)(2,1)S(1)}, u32[]{:S(2)}, u32[]{:S(2)}) %collective-permute-start.25) | collective-permute-done | bytes 655392 | tf_op jit(solution)/shard_map/ppermute | solution.py:27
  144.9 2.9 %collective-permute-start.27 = (bf16[40,2048]{1,0:T(8,128)(2,1)S(1)}, bf16[40,2048]{1,0:T(8,128)(2,1)S(1)}, u32[]{:S(2)}, u32[]{:S(2)}) collective-permute-start(bf16[40,2048]{1,0:T(8,128)(2,1)S(1)} %get-tuple-element.75), channel_id=1, source_target_pairs={{0,2},{1,3},{2,0},{3,1},{4,6},{5,7},{6,4},{7,5},{8,10},{9,11},{10,... | collective-permute-start | bytes 491528 | tf_op jit(solution)/shard_map/ppermute | solution.py:27
  148.3 2.5 %collective-permute-done.26 = bf16[40,2048]{1,0:T(8,128)(2,1)S(1)} collective-permute-done((bf16[40,2048]{1,0:T(8,128)(2,1)S(1)}, bf16[40,2048]{1,0:T(8,128)(2,1)S(1)}, u32[]{:S(2)}, u32[]{:S(2)}) %collective-permute-start.26) | collective-permute-done | bytes 163872 | tf_op jit(solution)/shard_map/ppermute | solution.py:27
  150.9 4.4 %collective-permute-done.27 = bf16[40,2048]{1,0:T(8,128)(2,1)S(1)} collective-permute-done((bf16[40,2048]{1,0:T(8,128)(2,1)S(1)}, bf16[40,2048]{1,0:T(8,128)(2,1)S(1)}, u32[]{:S(2)}, u32[]{:S(2)}) %collective-permute-start.27) | collective-permute-done | bytes 163872 | tf_op jit(solution)/shard_map/ppermute | solution.py:27
  (154 shorter events, 45.6 us)
Async XLA Ops:
  2.4 20.2 %all-to-all-start = ((bf16[16,48,128]{2,1,0:T(8,128)(2,1)}), bf16[16,48,128]{2,1,0:T(8,128)(2,1)S(1)}, u32[]{:S(2)}, u32[]{:S(2)}) async-start(bf16[16,48,128]{2,1,0:T(8,128)(2,1)} %bitcast.2), calls=%async_computation | async-start | bytes 393216 | tf_op jit(solution)/shard_map/all_to_all | solution.py:31
  22.6 35.1 %all-to-all-start.2 = ((bf16[16,32,896]{2,1,0:T(8,128)(2,1)}), bf16[16,32,896]{2,1,0:T(8,128)(2,1)}, u32[]{:S(2)}, u32[]{:S(2)}) async-start(bf16[16,32,896]{2,1,0:T(8,128)(2,1)} %bitcast.10), calls=%async_computation.2 | async-start | bytes 1835008 | tf_op jit(solution)/shard_map/all_to_all | solution.py:31
  27.0 14.4 %collective-permute-start = (bf16[160,2048]{1,0:T(8,128)(2,1)S(1)}, bf16[160,2048]{1,0:T(8,128)(2,1)S(1)}, u32[]{:S(2)}, u32[]{:S(2)}) collective-permute-start(bf16[160,2048]{1,0:T(8,128)(2,1)S(1)} %copy-done), channel_id=1, source_target_pairs={{0,4},{4,0},{1,5},{5,1},{2,6},{6,2},{3,7},{7,3},{8,12},{12,8},{9,1... | collective-permute-start | bytes 1966088 | tf_op jit(solution)/shard_map/ppermute | solution.py:27
  28.3 6.5 %collective-permute-start.3 = (bf16[8,96,128]{2,1,0:T(8,128)(2,1)S(1)}, bf16[8,96,128]{2,1,0:T(8,128)(2,1)S(1)}, u32[]{:S(2)}, u32[]{:S(2)}) collective-permute-start(bf16[8,96,128]{2,1,0:T(8,128)(2,1)S(1)} %bitcast.14), channel_id=1, source_target_pairs={{0,24},{8,0},{16,8},{24,16},{1,25},{9,1},{17,9},{25,17},{2,26},{10... | collective-permute-start | bytes 589832 | tf_op jit(solution)/shard_map/ppermute | solution.py:27
  31.1 8.0 %collective-permute-start.1 = (bf16[8,96,128]{2,1,0:T(8,128)(2,1)S(1)}, bf16[8,96,128]{2,1,0:T(8,128)(2,1)S(1)}, u32[]{:S(2)}, u32[]{:S(2)}) collective-permute-start(bf16[8,96,128]{2,1,0:T(8,128)(2,1)S(1)} %bitcast.15), channel_id=1, source_target_pairs={{0,8},{8,16},{16,24},{24,0},{1,9},{9,17},{17,25},{25,1},{2,10},{10... | collective-permute-start | bytes 589832 | tf_op jit(solution)/shard_map/ppermute | solution.py:27
  31.1 10.2 %collective-permute-start.2 = (bf16[8,96,128]{2,1,0:T(8,128)(2,1)S(1)}, bf16[8,96,128]{2,1,0:T(8,128)(2,1)S(1)}, u32[]{:S(2)}, u32[]{:S(2)}) collective-permute-start(bf16[8,96,128]{2,1,0:T(8,128)(2,1)S(1)} %bitcast.16), channel_id=1, source_target_pairs={{0,16},{8,24},{16,0},{24,8},{1,17},{9,25},{17,1},{25,9},{2,18},{10... | collective-permute-start | bytes 589832 | tf_op jit(solution)/shard_map/ppermute | solution.py:27
  44.7 4.9 %collective-permute-start.4 = (bf16[400,128]{1,0:T(8,128)(2,1)S(1)}, bf16[400,128]{1,0:T(8,128)(2,1)S(1)}, u32[]{:S(2)}, u32[]{:S(2)}) collective-permute-start(bf16[400,128]{1,0:T(8,128)(2,1)S(1)} %get-tuple-element.43.refs_0_), channel_id=1, source_target_pairs={{0,1},{1,2},{2,3},{3,0},{4,5},{5,6},{6,7},{7,4},{8,9},{9,10},{10,1... | collective-permute-start | bytes 307208 | tf_op jit(solution)/shard_map/ppermute | solution.py:27
  46.0 5.6 %collective-permute-start.5 = (bf16[400,128]{1,0:T(8,128)(2,1)S(1)}, bf16[400,128]{1,0:T(8,128)(2,1)S(1)}, u32[]{:S(2)}, u32[]{:S(2)}) collective-permute-start(bf16[400,128]{1,0:T(8,128)(2,1)S(1)} %get-tuple-element.43.refs_0_), channel_id=1, source_target_pairs={{0,2},{1,3},{2,0},{3,1},{4,6},{5,7},{6,4},{7,5},{8,10},{9,11},{10,... | collective-permute-start | bytes 307208 | tf_op jit(solution)/shard_map/ppermute | solution.py:27
  53.7 7.8 %collective-permute-start.7 = (bf16[1600,128]{1,0:T(8,128)(2,1)}, bf16[1600,128]{1,0:T(8,128)(2,1)}, u32[]{:S(2)}, u32[]{:S(2)}) collective-permute-start(bf16[1600,128]{1,0:T(8,128)(2,1)} %pad_maximum_fusion), channel_id=1, source_target_pairs={{0,4},{4,0},{1,5},{5,1},{2,6},{6,2},{3,7},{7,3},{8,12},{12,8},{9,1... | collective-permute-start | bytes 1228808 | tf_op jit(solution)/shard_map/ppermute | solution.py:27
  58.7 14.8 %collective-permute-start.18 = (bf16[8,64,512]{2,1,0:T(8,128)(2,1)S(1)}, bf16[8,64,512]{2,1,0:T(8,128)(2,1)S(1)}, u32[]{:S(2)}, u32[]{:S(2)}) collective-permute-start(bf16[8,64,512]{2,1,0:T(8,128)(2,1)S(1)} %slice.35.a0), channel_id=1, source_target_pairs={{0,8},{8,16},{16,24},{24,0},{1,9},{9,17},{17,25},{25,1},{2,10},{10... | collective-permute-start | bytes 1572872 | tf_op jit(solution)/shard_map/ppermute | solution.py:27
  58.8 16.7 %collective-permute-start.19 = (bf16[8,64,512]{2,1,0:T(8,128)(2,1)S(1)}, bf16[8,64,512]{2,1,0:T(8,128)(2,1)S(1)}, u32[]{:S(2)}, u32[]{:S(2)}) collective-permute-start(bf16[8,64,512]{2,1,0:T(8,128)(2,1)S(1)} %slice.35.a0), channel_id=1, source_target_pairs={{0,24},{8,0},{16,8},{24,16},{1,25},{9,1},{17,9},{25,17},{2,26},{10... | collective-permute-start | bytes 1572872 | tf_op jit(solution)/shard_map/ppermute | solution.py:27
  68.6 11.7 %collective-permute-start.8 = (bf16[800,128]{1,0:T(8,128)(2,1)}, bf16[800,128]{1,0:T(8,128)(2,1)}, u32[]{:S(2)}, u32[]{:S(2)}) collective-permute-start(bf16[800,128]{1,0:T(8,128)(2,1)} %get-tuple-element.52.refs_1_), channel_id=1, source_target_pairs={{0,32},{32,64},{64,96},{96,128},{128,160},{160,192},{192,224},{224... | collective-permute-start | bytes 614408 | tf_op jit(solution)/shard_map/ppermute | solution.py:27
  69.9 17.1 %all-to-all-start.1 = ((bf16[4,480,128]{2,1,0:T(8,128)(2,1)}), bf16[4,480,128]{2,1,0:T(8,128)(2,1)S(1)}, u32[]{:S(2)}, u32[]{:S(2)}) async-start(bf16[4,480,128]{2,1,0:T(8,128)(2,1)} %copy-done.4), calls=%async_computation.1 | async-start | bytes 983040 | tf_op jit(solution)/shard_map/all_to_all | solution.py:31
  74.2 13.0 %collective-permute-start.20 = (bf16[4,64,512]{2,1,0:T(8,128)(2,1)}, bf16[4,64,512]{2,1,0:T(8,128)(2,1)}, u32[]{:S(2)}, u32[]{:S(2)}) collective-permute-start(bf16[4,64,512]{2,1,0:T(8,128)(2,1)} %slice.36), channel_id=1, source_target_pairs={{0,8},{8,16},{16,24},{24,0},{1,9},{9,17},{17,25},{25,1},{2,10},{10... | collective-permute-start | bytes 786440 | tf_op jit(solution)/shard_map/ppermute | solution.py:27
  76.3 10.9 %collective-permute-start.21 = (bf16[4,64,512]{2,1,0:T(8,128)(2,1)}, bf16[4,64,512]{2,1,0:T(8,128)(2,1)}, u32[]{:S(2)}, u32[]{:S(2)}) collective-permute-start(bf16[4,64,512]{2,1,0:T(8,128)(2,1)} %slice.37), channel_id=1, source_target_pairs={{0,24},{8,0},{16,8},{24,16},{1,25},{9,1},{17,9},{25,17},{2,26},{10... | collective-permute-start | bytes 786440 | tf_op jit(solution)/shard_map/ppermute | solution.py:27
  77.6 6.0 %collective-permute-start.9 = (bf16[800,128]{1,0:T(8,128)(2,1)}, bf16[800,128]{1,0:T(8,128)(2,1)}, u32[]{:S(2)}, u32[]{:S(2)}) collective-permute-start(bf16[800,128]{1,0:T(8,128)(2,1)} %get-tuple-element.52.refs_1_), channel_id=1, source_target_pairs={{0,224},{32,0},{64,32},{96,64},{128,96},{160,128},{192,160},{224,1... | collective-permute-start | bytes 614408 | tf_op jit(solution)/shard_map/ppermute | solution.py:27
  80.3 6.7 %collective-permute-start.10 = (bf16[800,128]{1,0:T(8,128)(2,1)}, bf16[800,128]{1,0:T(8,128)(2,1)}, u32[]{:S(2)}, u32[]{:S(2)}) collective-permute-start(bf16[800,128]{1,0:T(8,128)(2,1)} %collective-permute-done.8.refs_2_), channel_id=1, source_target_pairs={{0,32},{32,64},{64,96},{96,128},{128,160},{160,192},{192,224},{224... | collective-permute-start | bytes 614408 | tf_op jit(solution)/shard_map/ppermute | solution.py:27
  83.6 12.8 %collective-permute-start.11 = (bf16[800,128]{1,0:T(8,128)(2,1)}, bf16[800,128]{1,0:T(8,128)(2,1)}, u32[]{:S(2)}, u32[]{:S(2)}) collective-permute-start(bf16[800,128]{1,0:T(8,128)(2,1)} %collective-permute-done.9.refs_3_), channel_id=1, source_target_pairs={{0,224},{32,0},{64,32},{96,64},{128,96},{160,128},{192,160},{224,1... | collective-permute-start | bytes 614408 | tf_op jit(solution)/shard_map/ppermute | solution.py:27
  87.0 12.0 %collective-permute-start.12 = (bf16[800,128]{1,0:T(8,128)(2,1)}, bf16[800,128]{1,0:T(8,128)(2,1)}, u32[]{:S(2)}, u32[]{:S(2)}) collective-permute-start(bf16[800,128]{1,0:T(8,128)(2,1)} %collective-permute-done.10.refs_4_), channel_id=1, source_target_pairs={{0,32},{32,64},{64,96},{96,128},{128,160},{160,192},{192,224},{224... | collective-permute-start | bytes 614408 | tf_op jit(solution)/shard_map/ppermute | solution.py:27
  92.9 9.0 %all-to-all-start.3 = ((bf16[4,272,128]{2,1,0:T(8,128)(2,1)}), bf16[4,272,128]{2,1,0:T(8,128)(2,1)S(1)}, u32[]{:S(2)}, u32[]{:S(2)}) async-start(bf16[4,272,128]{2,1,0:T(8,128)(2,1)} %copy-done.9), calls=%async_computation.3 | async-start | bytes 557056 | tf_op jit(solution)/shard_map/all_to_all | solution.py:31
  96.4 17.2 %collective-permute-start.13 = (bf16[800,128]{1,0:T(8,128)(2,1)}, bf16[800,128]{1,0:T(8,128)(2,1)}, u32[]{:S(2)}, u32[]{:S(2)}) collective-permute-start(bf16[800,128]{1,0:T(8,128)(2,1)} %collective-permute-done.11.refs_5_), channel_id=1, source_target_pairs={{0,224},{32,0},{64,32},{96,64},{128,96},{160,128},{192,160},{224,1... | collective-permute-start | bytes 614408 | tf_op jit(solution)/shard_map/ppermute | solution.py:27
  99.0 14.6 %collective-permute-start.14 = (bf16[800,128]{1,0:T(8,128)(2,1)}, bf16[800,128]{1,0:T(8,128)(2,1)}, u32[]{:S(2)}, u32[]{:S(2)}) collective-permute-start(bf16[800,128]{1,0:T(8,128)(2,1)} %collective-permute-done.12.refs_6_), channel_id=1, source_target_pairs={{0,32},{32,64},{64,96},{96,128},{128,160},{160,192},{192,224},{224... | collective-permute-start | bytes 614408 | tf_op jit(solution)/shard_map/ppermute | solution.py:27
  103.4 28.2 %all-to-all-start.4 = ((bf16[8,144,128]{2,1,0:T(8,128)(2,1)}), bf16[8,144,128]{2,1,0:T(8,128)(2,1)}, u32[]{:S(2)}, u32[]{:S(2)}) async-start(bf16[8,144,128]{2,1,0:T(8,128)(2,1)} %get-tuple-element.60), calls=%async_computation.4 | async-start | bytes 589824 | tf_op jit(solution)/shard_map/all_to_all | solution.py:31
  110.7 11.8 %collective-permute-start.22 = (bf16[8,64,384]{2,1,0:T(8,128)(2,1)S(1)}, bf16[8,64,384]{2,1,0:T(8,128)(2,1)S(1)}, u32[]{:S(2)}, u32[]{:S(2)}) collective-permute-start(bf16[8,64,384]{2,1,0:T(8,128)(2,1)S(1)} %slice.38.l0.o0), channel_id=1, source_target_pairs={{0,8},{8,16},{16,24},{24,0},{1,9},{9,17},{17,25},{25,1},{2,10},{10... | collective-permute-start | bytes 1179656 | tf_op jit(solution)/shard_map/ppermute | solution.py:27
  111.1 16.3 %collective-permute-start.23 = (bf16[8,64,384]{2,1,0:T(8,128)(2,1)S(1)}, bf16[8,64,384]{2,1,0:T(8,128)(2,1)S(1)}, u32[]{:S(2)}, u32[]{:S(2)}) collective-permute-start(bf16[8,64,384]{2,1,0:T(8,128)(2,1)S(1)} %slice.38.l0.o0), channel_id=1, source_target_pairs={{0,16},{8,24},{16,0},{24,8},{1,17},{9,25},{17,1},{25,9},{2,18},{10... | collective-permute-start | bytes 1179656 | tf_op jit(solution)/shard_map/ppermute | solution.py:27
  113.0 18.6 %collective-permute-start.24 = (bf16[8,64,384]{2,1,0:T(8,128)(2,1)S(1)}, bf16[8,64,384]{2,1,0:T(8,128)(2,1)S(1)}, u32[]{:S(2)}, u32[]{:S(2)}) collective-permute-start(bf16[8,64,384]{2,1,0:T(8,128)(2,1)S(1)} %slice.38.l0.o0), channel_id=1, source_target_pairs={{0,24},{8,0},{16,8},{24,16},{1,25},{9,1},{17,9},{25,17},{2,26},{10... | collective-permute-start | bytes 1179656 | tf_op jit(solution)/shard_map/ppermute | solution.py:27
  120.3 17.7 %collective-permute-start.15 = (bf16[336,128]{1,0:T(8,128)(2,1)}, bf16[336,128]{1,0:T(8,128)(2,1)S(1)}, u32[]{:S(2)}, u32[]{:S(2)}) collective-permute-start(bf16[336,128]{1,0:T(8,128)(2,1)} %get-tuple-element.54), channel_id=1, source_target_pairs={{0,8},{8,16},{16,24},{24,0},{1,9},{9,17},{17,25},{25,1},{2,10},{10... | collective-permute-start | bytes 258056 | tf_op jit(solution)/shard_map/ppermute | solution.py:27
  121.2 16.9 %collective-permute-start.16 = (bf16[336,128]{1,0:T(8,128)(2,1)}, bf16[336,128]{1,0:T(8,128)(2,1)S(1)}, u32[]{:S(2)}, u32[]{:S(2)}) collective-permute-start(bf16[336,128]{1,0:T(8,128)(2,1)} %get-tuple-element.55), channel_id=1, source_target_pairs={{0,16},{8,24},{16,0},{24,8},{1,17},{9,25},{17,1},{25,9},{2,18},{10... | collective-permute-start | bytes 258056 | tf_op jit(solution)/shard_map/ppermute | solution.py:27
  122.6 15.5 %collective-permute-start.17 = (bf16[336,128]{1,0:T(8,128)(2,1)}, bf16[336,128]{1,0:T(8,128)(2,1)S(1)}, u32[]{:S(2)}, u32[]{:S(2)}) collective-permute-start(bf16[336,128]{1,0:T(8,128)(2,1)} %get-tuple-element.56), channel_id=1, source_target_pairs={{0,24},{8,0},{16,8},{24,16},{1,25},{9,1},{17,9},{25,17},{2,26},{10... | collective-permute-start | bytes 258056 | tf_op jit(solution)/shard_map/ppermute | solution.py:27
  144.2 6.7 %collective-permute-start.26 = (bf16[40,2048]{1,0:T(8,128)(2,1)S(1)}, bf16[40,2048]{1,0:T(8,128)(2,1)S(1)}, u32[]{:S(2)}, u32[]{:S(2)}) collective-permute-start(bf16[40,2048]{1,0:T(8,128)(2,1)S(1)} %get-tuple-element.73), channel_id=1, source_target_pairs={{0,1},{1,2},{2,3},{3,0},{4,5},{5,6},{6,7},{7,4},{8,9},{9,10},{10,1... | collective-permute-start | bytes 491528 | tf_op jit(solution)/shard_map/ppermute | solution.py:27
  144.9 10.3 %collective-permute-start.27 = (bf16[40,2048]{1,0:T(8,128)(2,1)S(1)}, bf16[40,2048]{1,0:T(8,128)(2,1)S(1)}, u32[]{:S(2)}, u32[]{:S(2)}) collective-permute-start(bf16[40,2048]{1,0:T(8,128)(2,1)S(1)} %get-tuple-element.75), channel_id=1, source_target_pairs={{0,2},{1,3},{2,0},{3,1},{4,6},{5,7},{6,4},{7,5},{8,10},{9,11},{10,... | collective-permute-start | bytes 491528 | tf_op jit(solution)/shard_map/ppermute | solution.py:27
  147.8 7.4 %collective-permute-start.28 = (bf16[40,2048]{1,0:T(8,128)(2,1)S(1)}, bf16[40,2048]{1,0:T(8,128)(2,1)S(1)}, u32[]{:S(2)}, u32[]{:S(2)}) collective-permute-start(bf16[40,2048]{1,0:T(8,128)(2,1)S(1)} %get-tuple-element.74), channel_id=1, source_target_pairs={{0,3},{1,0},{2,1},{3,2},{4,7},{5,4},{6,5},{7,6},{8,11},{9,8},{10,9... | collective-permute-start | bytes 491528 | tf_op jit(solution)/shard_map/ppermute | solution.py:27
  (48 other events, 251.4 us)
where the time goes:
time: 158 us; the launch traced here: 156 us
  starting transfers between devices  70.6 us (45%)
  waiting for transfers between devices  36.6 us (23%)
  local copies, waits for them, and re-layouts  23.1 us (15%)
  Pallas kernels  22 us (14%)
  other arithmetic  3.25 us (2%)
    ppermute x29, starting transfers between devices, shift(): lax.ppermute(value, axis, [(i, (i + by) % count) for i in range(count)])  43.1 us
    ppermute x29, waiting for transfers between devices, shift(): lax.ppermute(value, axis, [(i, (i + by) % count) for i in range(count)])  29.6 us
    all_to_all x5, starting transfers between devices, exchange(): return lax.all_to_all(value, axis, 0, 0, tiled=True)  27.5 us
    pallas_call x10, Pallas kernels, call(): pl.pallas_call(body, out_shape=outs, grid=grid, in_specs=[whole if specs...  22 us
    unnamed x92, local copies, waits for them, and re-layouts  19.3 us
    all_to_all x5, waiting for transfers between devices, exchange(): return lax.all_to_all(value, axis, 0, 0, tiled=True)  7.03 us
  transfers between devices with their start and end apart: 34, of which 15 were waited for; matrix products, arithmetic and copies ran while one was open for 4% of the time, Pallas kernels for 13%

commit v1 on v0

--- a/solution.py
+++ b/solution.py
@@ -113,12 +113,14 @@
             out[k, j, :, :] = ready
 
 
-def prep_kernel(after, cq, fg, bg, cv, og, co, ao, out):
+def prep_kernel(after, cq, fg, bg, cv, og, co, ao, out_a, out_l):
     for j in range(NC):
         lanes = slice(j * HEAD, (j + 1) * HEAD)
         for k in range(NZ):
-            for i, w in enumerate((cq, fg, bg, cv, og, co, ao)):
-                out[k, j, :, i * HEAD : (i + 1) * HEAD] = w[:, lanes]
+            for i, w in enumerate((cq, fg, bg, cv)):
+                out_a[k, j, :, i * HEAD : (i + 1) * HEAD] = w[:, lanes]
+            for i, w in enumerate((og, co, ao)):
+                out_l[k, j, :, i * HEAD : (i + 1) * HEAD] = w[:, lanes]
 
 
 def ups_kernel(q_up, kv_up, q_gain, kv_gain, wq, wkv, gq, gkv):
@@ -204,8 +206,7 @@
     a3,
     a4,
     inside,
-    probe_f,
-    probe_b,
+    probes,
     packet,
     w_scr,
     sems,
@@ -232,7 +233,7 @@
         total = cum[n - 1 : n, :] if d == 0 else cum[0:1, :]
         probe = (query * jnp.exp(cum)).astype(BF)
         look = (key * jnp.exp(-cum)).astype(BF)
-        (probe_f if d == 0 else probe_b)[...] = probe
+        probes[d] = probe
         score = jnp.where(keep, dot_nt(probe, look), 0.0)
         within = score if within is None else within + score
         digest = dot_tn(payload, (key * jnp.exp(total - cum)).astype(BF)).astype(BF)
@@ -260,7 +261,7 @@
     return state, log
 
 
-def slab_kernel(slab, state_f, state_b, log_out, send):
+def slab_kernel(slab, nears, log_out, send):
     z, y = lax.axis_index("z"), lax.axis_index("y")
     at = lax.broadcasted_iota(jnp.int32, (16, HEAD), 0)
     kept = []
@@ -276,7 +277,7 @@
 
         part, log = walk(states, logs, order, (lambda j: j < y) if d == 0 else (lambda j: j > y))
         full, full_log = walk(states, logs, order, lambda j: j >= 0)
-        (state_f if d == 0 else state_b)[...] = part
+        nears[d] = part
         log_out[d : d + 1, :] = log
         high = full_log.astype(BF).astype(F32)
         tail = jnp.where(at == 0, high, jnp.where(at == 1, full_log - high, 0.0)).astype(BF)
@@ -289,11 +290,9 @@
 
 def close_kernel(
     outer,
-    state_f,
-    state_b,
+    nears,
     log_in,
-    probe_f,
-    probe_b,
+    probes,
     inside,
     gain,
     normed,
@@ -319,10 +318,8 @@
             return block[0:1, :] + block[1:2, :]
 
         far, _ = walk(states, logs, order, (lambda j: j < z) if d == 0 else (lambda j: j > z))
-        near = (state_f if d == 0 else state_b)[...]
-        state = near + far * jnp.exp(log_in[d : d + 1, :])
-        probe = (probe_f if d == 0 else probe_b)[...]
-        combined = combined + dot_nt(probe, state.astype(BF))
+        state = nears[d] + far * jnp.exp(log_in[d : d + 1, :])
+        combined = combined + dot_nt(probes[d], state.astype(BF))
     opened = dot(normed[...], gathered(w_scr, copies)).astype(BF).astype(F32)
     opened = opened * jax.nn.sigmoid(opened)
     scale = inverse_rms(squares(combined), HEAD)
@@ -500,9 +497,9 @@
         prep_low_kernel, made((NZ, NC, piece * 3 // 2, HEAD), BF), (query_down, latent_down)
     )
     anywhere = pl.BlockSpec(memory_space=pl.ANY)
-    send_a = call(
+    send_a, send_l = call(
         prep_kernel,
-        made((NZ, NC, piece, 896), BF),
+        [made((NZ, NC, piece, 512), BF), made((NZ, NC, piece, 384), BF)],
         (
             send_b,
             chain_query,
@@ -523,10 +520,9 @@
     other = shift(tokens, "c", NC, 1)
     column_b = along_z(send_b)
     column_a = along_z(send_a)
-    column_a, column_l = column_a[:, :, :512], column_a[:, :, 512:]
+    column_l = along_z(send_l)
     weights_b = [column_b] + [shift(column_b, "y", NY, k) for k in range(1, NY)]
     weights_a = spread_y(column_a)
-    weights_l = [column_l] + [shift(column_l, "y", NY, k) for k in range(1, NY)]
 
     positions = ((z * NY + y) * n + jnp.arange(n, dtype=jnp.int32)).astype(F32)
     inverse = THETA ** (-jnp.arange(0, ROPE, 2).astype(F32) / ROPE)
@@ -574,29 +570,28 @@
         flops=2 * n * (QLAT * QK + KVLAT * 256),
     )
     kv = ring_z(kv_piece)
+    queries, column_l = lax.optimization_barrier((queries, column_l))
     all_queries = exchange(queries, "y")
-    part = attend(all_queries, kv)
-    parts = [part[0]] + [shift(part[k], "y", NY, k) for k in range(1, NY)]
-
-    inside, probe_f, probe_b, packet = call(
+    weights_l = [column_l] + [shift(column_l, "y", NY, k) for k in range(1, NY)]
+
+    inside, probes, packet = call(
         chain_kernel,
         [
             made((n, HEAD), F32),
-            made((n, HEAD), BF),
-            made((n, HEAD), BF),
+            made((2, n, HEAD), BF),
             made((NY, 2 * HEAD + 16, HEAD), BF),
         ],
-        [all_queries, rates, normed] + weights_a,
+        [kv_piece, rates, normed] + weights_a,
         scratch=[pltpu.VMEM((NZ, NY, NC * piece, 512), BF), pltpu.SemaphoreType.DMA((5,))],
         specs=[anywhere, None, None] + [anywhere] * 5,
         flops=2 * n * width * 512,
     )
+    packet, all_queries = lax.optimization_barrier((packet, all_queries))
     slab = exchange(packet, "y")
-    state_f, state_b, log_in, send = call(
+    nears, log_in, send = call(
         slab_kernel,
         [
-            made((HEAD, HEAD), F32),
-            made((HEAD, HEAD), F32),
+            made((2, HEAD, HEAD), F32),
             made((2, HEAD), F32),
             made((NZ, HEAD + 16, HEAD), BF),
         ],
@@ -604,23 +599,23 @@
     )
     outer = exchange(send, "z")
 
+    part = attend(all_queries, kv)
+    parts = [part[0]] + [shift(part[k], "y", NY, k) for k in range(1, NY)]
     chain_mixed = call(
         close_kernel,
         made((n, HEAD), BF),
         (
             outer,
-            state_f,
-            state_b,
+            nears,
             log_in,
-            probe_f,
-            probe_b,
+            probes,
             inside,
             gain_c,
             normed,
             *weights_l,
         ),
         scratch=[pltpu.VMEM((NZ, NY, NC * piece, HEAD), BF), pltpu.SemaphoreType.DMA((4,))],
-        specs=[None] * 9 + [anywhere] * 4,
+        specs=[None] * 7 + [anywhere] * 4,
     )
     mine, theirs = call(
         final_kernel,

time: 158 us -> 160 us (1.013)
  starting transfers between devices: 70.6 us -> 74.2 us
  local copies, waits for them, and re-layouts: 23.1 us -> 24.9 us
    all_to_all x5 -> x6, starting transfers between devices: 27.5 us -> 37.5 us  [exchange(): return lax.all_to_all(value, axis, 0, 0, tiled=True)]
    ppermute x29, starting transfers between devices: 43.1 us -> 36.7 us  [shift(): lax.ppermute(value, axis, [(i, (i + by) % count) for i in range(count)])]
    unnamed x92 -> x96, local copies, waits for them, and re-layouts: 19.3 us -> 24.1 us
    slice x2 -> x0, local copies, waits for them, and re-layouts: 2.12 us -> none  [on_device(): column_a, column_l = (column_a[:, :, :512], column_a[:, :, 512:])]
    ppermute x29, waiting for transfers between devices: 29.6 us -> 27.9 us  [shift(): lax.ppermute(value, axis, [(i, (i + by) % count) for i in range(count)])]
    all_to_all x5 -> x6, waiting for transfers between devices: 7.03 us -> 7.39 us  [exchange(): return lax.all_to_all(value, axis, 0, 0, tiled=True)]
  transfers between devices with their start and end apart: 34 -> 35, of which waited for: 15 -> 12; matrix products, arithmetic and copies ran while one was open for 4% -> 2% of each run, Pallas kernels for 13% -> 11%
where the time goes in v1:
time: 160 us; the launch traced here: 158 us
  starting transfers between devices  74.2 us (46%)
  waiting for transfers between devices  35.3 us (22%)
  local copies, waits for them, and re-layouts  24.9 us (16%)
  Pallas kernels  20.6 us (13%)
  other arithmetic  2.61 us (2%)
    all_to_all x6, starting transfers between devices, exchange(): return lax.all_to_all(value, axis, 0, 0, tiled=True)  37.5 us
    ppermute x29, starting transfers between devices, shift(): lax.ppermute(value, axis, [(i, (i + by) % count) for i in range(count)])  36.7 us
    ppermute x29, waiting for transfers between devices, shift(): lax.ppermute(value, axis, [(i, (i + by) % count) for i in range(count)])  27.9 us
    unnamed x96, local copies, waits for them, and re-layouts  24.1 us
    pallas_call x10, Pallas kernels, call(): pl.pallas_call(body, out_shape=outs, grid=grid, in_specs=[whole if specs...  20.6 us
    all_to_all x6, waiting for transfers between devices, exchange(): return lax.all_to_all(value, axis, 0, 0, tiled=True)  7.39 us
  transfers between devices with their start and end apart: 35, of which 12 were waited for; matrix products, arithmetic and copies ran while one was open for 2% of the time, Pallas kernels for 11%

profile of v1, /device:TPU:1, one launch (start us, length us, event | category | flops | bytes accessed | tf_op | source)
XLA Modules:
  0.0 158.0 jit_solution(7777480204899832667)
XLA Ops:
  2.5 10.0 %all-to-all-start = ((bf16[16,48,128]{2,1,0:T(8,128)(2,1)}), bf16[16,48,128]{2,1,0:T(8,128)(2,1)S(1)}, u32[]{:S(2)}, u32[]{:S(2)}) async-start(bf16[16,48,128]{2,1,0:T(8,128)(2,1)} %bitcast.2), calls=%async_computation | async-start | bytes 393216 | tf_op jit(solution)/shard_map/all_to_all | solution.py:31
  19.2 3.5 %all-to-all-done = bf16[16,48,128]{2,1,0:T(8,128)(2,1)S(1)} async-done(((bf16[16,48,128]{2,1,0:T(8,128)(2,1)}), bf16[16,48,128]{2,1,0:T(8,128)(2,1)S(1)}, u32[]{:S(2)}, u32[]{:S(2)}) %all-to-all-start) | async-done | bytes 196640 | tf_op jit(solution)/shard_map/all_to_all | solution.py:31
  22.7 3.9 %all-to-all-start.1 = ((bf16[16,32,512]{2,1,0:T(8,128)(2,1)}), bf16[16,32,512]{2,1,0:T(8,128)(2,1)S(1)}, u32[]{:S(2)}, u32[]{:S(2)}) async-start(bf16[16,32,512]{2,1,0:T(8,128)(2,1)} %bitcast.10), calls=%async_computation.1 | async-start | bytes 1048576 | tf_op jit(solution)/shard_map/all_to_all | solution.py:31
  28.0 2.8 %collective-permute-start.3 = (bf16[8,96,128]{2,1,0:T(8,128)(2,1)S(1)}, bf16[8,96,128]{2,1,0:T(8,128)(2,1)S(1)}, u32[]{:S(2)}, u32[]{:S(2)}) collective-permute-start(bf16[8,96,128]{2,1,0:T(8,128)(2,1)S(1)} %bitcast.24), channel_id=1, source_target_pairs={{0,24},{8,0},{16,8},{24,16},{1,25},{9,1},{17,9},{25,17},{2,26},{10... | collective-permute-start | bytes 589832 | tf_op jit(solution)/shard_map/ppermute | solution.py:27
  30.8 1.6 %collective-permute-start.2 = (bf16[8,96,128]{2,1,0:T(8,128)(2,1)S(1)}, bf16[8,96,128]{2,1,0:T(8,128)(2,1)S(1)}, u32[]{:S(2)}, u32[]{:S(2)}) collective-permute-start(bf16[8,96,128]{2,1,0:T(8,128)(2,1)S(1)} %bitcast.26), channel_id=1, source_target_pairs={{0,16},{8,24},{16,0},{24,8},{1,17},{9,25},{17,1},{25,9},{2,18},{10... | collective-permute-start | bytes 589832 | tf_op jit(solution)/shard_map/ppermute | solution.py:27
  34.5 4.3 %collective-permute-done.1.b1 = bf16[8,96,128]{2,1,0:T(8,128)(2,1)S(1)} collective-permute-done((bf16[8,96,128]{2,1,0:T(8,128)(2,1)S(1)}, bf16[8,96,128]{2,1,0:T(8,128)(2,1)S(1)}, u32[]{:S(2)}, u32[]{:S(2)}) %collective-permute-start.1) | collective-permute-done | bytes 196640 | tf_op jit(solution)/shard_map/ppermute | solution.py:27
  38.8 2.2 %collective-permute-done.2.b2 = bf16[8,96,128]{2,1,0:T(8,128)(2,1)S(1)} collective-permute-done((bf16[8,96,128]{2,1,0:T(8,128)(2,1)S(1)}, bf16[8,96,128]{2,1,0:T(8,128)(2,1)S(1)}, u32[]{:S(2)}, u32[]{:S(2)}) %collective-permute-start.2) | collective-permute-done | bytes 196640 | tf_op jit(solution)/shard_map/ppermute | solution.py:27
  42.0 3.3 %shard_map.201 = (bf16[320,2048]{1,0:T(8,128)(2,1)S(1)}, bf16[400,128]{1,0:T(8,128)(2,1)S(1)}, bf16[320,64]{1,0:T(8,128)(2,1)S(1)}) custom-call(bf16[160,2048]{1,0:T(8,128)(2,1)S(1)} %copy-done, bf16[160,2048]{1,0:T(8,128)(2,1)S(1)} %collective-permute-done.other, f32[1,2048]{1,0:T(1,128)S(1)} %bitcast.32, bf16[64,2048]{1,0:T(8,128)(2,1)S(1)} %bitcast.29, ...), custom_call_target="tpu_custom_call" | custom-call | flops 419430400 | bytes 1048576 | tf_op jit(solution)/shard_map/pallas_call | solution.py:77
  47.1 2.5 %collective-permute-start.5 = (bf16[400,128]{1,0:T(8,128)(2,1)S(1)}, bf16[400,128]{1,0:T(8,128)(2,1)S(1)}, u32[]{:S(2)}, u32[]{:S(2)}) collective-permute-start(bf16[400,128]{1,0:T(8,128)(2,1)S(1)} %get-tuple-element.47.refs_0_), channel_id=1, source_target_pairs={{0,2},{1,3},{2,0},{3,1},{4,6},{5,7},{6,4},{7,5},{8,10},{9,11},{10,... | collective-permute-start | bytes 307208 | tf_op jit(solution)/shard_map/ppermute | solution.py:27
  50.7 10.5 %all-to-all-start.2 = ((bf16[16,32,384]{2,1,0:T(8,128)(2,1)}), bf16[16,32,384]{2,1,0:T(8,128)(2,1)S(1)}, u32[]{:S(2)}, u32[]{:S(2)}) async-start(bf16[16,32,384]{2,1,0:T(8,128)(2,1)} %bitcast.28), calls=%async_computation.2 | async-start | bytes 786432 | tf_op jit(solution)/shard_map/all_to_all | solution.py:31
  62.0 2.7 %collective-permute-start.9 = (bf16[8,64,512]{2,1,0:T(8,128)(2,1)S(1)}, bf16[8,64,512]{2,1,0:T(8,128)(2,1)S(1)}, u32[]{:S(2)}, u32[]{:S(2)}) collective-permute-start(bf16[8,64,512]{2,1,0:T(8,128)(2,1)S(1)} %bitcast.22), channel_id=1, source_target_pairs={{0,24},{8,0},{16,8},{24,16},{1,25},{9,1},{17,9},{25,17},{2,26},{10... | collective-permute-start | bytes 1572872 | tf_op jit(solution)/shard_map/ppermute | solution.py:27
  73.1 2.3 %shard_map.202 = (bf16[4,480,128]{2,1,0:T(8,128)(2,1)S(1)}, bf16[800,128]{1,0:T(8,128)(2,1)}) custom-call(bf16[400,128]{1,0:T(8,128)(2,1)S(1)} %get-tuple-element.47.refs_0_, bf16[400,128]{1,0:T(8,128)(2,1)S(1)} %copy-done.7, bf16[400,128]{1,0:T(8,128)(2,1)S(1)} %copy-done.9, bf16[400,128]{1,0:T(8,128)(2,1)S(1)} %copy-done.11, ...), custom_call_target="tpu_custom_call" | custom-call | flops 178257920 | bytes 1048576 | tf_op jit(solution)/shard_map/pallas_call | solution.py:77
  77.6 4.1 %all-to-all-start.3 = ((bf16[4,480,128]{2,1,0:T(8,128)(2,1)}), bf16[4,480,128]{2,1,0:T(8,128)(2,1)}, u32[]{:S(2)}, u32[]{:S(2)}) async-start(bf16[4,480,128]{2,1,0:T(8,128)(2,1)} %copy-done.5), calls=%async_computation.3 | async-start | bytes 983040 | tf_op jit(solution)/shard_map/all_to_all | solution.py:31
  81.8 1.5 collective-permute-start.10
  86.8 3.0 %collective-permute-done.13.refs_3_ = bf16[800,128]{1,0:T(8,128)(2,1)} collective-permute-done((bf16[800,128]{1,0:T(8,128)(2,1)}, bf16[800,128]{1,0:T(8,128)(2,1)}, u32[]{:S(2)}, u32[]{:S(2)}) %collective-permute-start.13) | collective-permute-done | bytes 204832 | tf_op jit(solution)/shard_map/ppermute | solution.py:27
  89.8 2.8 %collective-permute-start.15 = (bf16[800,128]{1,0:T(8,128)(2,1)}, bf16[800,128]{1,0:T(8,128)(2,1)}, u32[]{:S(2)}, u32[]{:S(2)}) collective-permute-start(bf16[800,128]{1,0:T(8,128)(2,1)} %collective-permute-done.13.refs_3_), channel_id=1, source_target_pairs={{0,224},{32,0},{64,32},{96,64},{128,96},{160,128},{192,160},{224,1... | collective-permute-start | bytes 614408 | tf_op jit(solution)/shard_map/ppermute | solution.py:27
  92.6 2.4 %collective-permute-done.10.a3 = bf16[4,64,512]{2,1,0:T(8,128)(2,1)S(1)} collective-permute-done((bf16[4,64,512]{2,1,0:T(8,128)(2,1)S(1)}, bf16[4,64,512]{2,1,0:T(8,128)(2,1)S(1)}, u32[]{:S(2)}, u32[]{:S(2)}) %collective-permute-start.10) | collective-permute-done | bytes 262176 | tf_op jit(solution)/shard_map/ppermute | solution.py:27
  95.0 2.8 %shard_map.204 = (f32[320,128]{1,0:T(8,128)S(1)}, bf16[2,320,128]{2,1,0:T(8,128)(2,1)S(1)}, bf16[4,272,128]{2,1,0:T(8,128)(2,1)}) custom-call(bf16[800,128]{1,0:T(8,128)(2,1)} %get-tuple-element.55.after.refs_1_, f32[2,128]{1,0:T(2,128)S(1)} %dynamic-slice_multiply_fusion.rates, bf16[320,2048]{1,0:T(8,128)(2,1)S(1)} %get-tuple-element.57.normed, ...), custom_call_target="tpu_custom_call" | custom-call | flops 671088640 | bytes 1048576 | tf_op jit(solution)/shard_map/pallas_call | solution.py:77
  98.4 3.5 %all-to-all-start.4 = ((bf16[4,272,128]{2,1,0:T(8,128)(2,1)}), bf16[4,272,128]{2,1,0:T(8,128)(2,1)S(1)}, u32[]{:S(2)}, u32[]{:S(2)}) async-start(bf16[4,272,128]{2,1,0:T(8,128)(2,1)} %get-tuple-element.68), calls=%async_computation.4 | async-start | bytes 557056 | tf_op jit(solution)/shard_map/all_to_all | solution.py:31
  101.9 1.7 %collective-permute-start.17 = (bf16[800,128]{1,0:T(8,128)(2,1)}, bf16[800,128]{1,0:T(8,128)(2,1)}, u32[]{:S(2)}, u32[]{:S(2)}) collective-permute-start(bf16[800,128]{1,0:T(8,128)(2,1)} %collective-permute-done.15.refs_5_), channel_id=1, source_target_pairs={{0,224},{32,0},{64,32},{96,64},{128,96},{160,128},{192,160},{224,1... | collective-permute-start | bytes 614408 | tf_op jit(solution)/shard_map/ppermute | solution.py:27
  103.6 3.9 %all-to-all-done.4.slab = bf16[4,272,128]{2,1,0:T(8,128)(2,1)S(1)} async-done(((bf16[4,272,128]{2,1,0:T(8,128)(2,1)}), bf16[4,272,128]{2,1,0:T(8,128)(2,1)S(1)}, u32[]{:S(2)}, u32[]{:S(2)}) %all-to-all-start.4) | async-done | bytes 278560 | tf_op jit(solution)/shard_map/all_to_all | solution.py:31
  109.0 5.6 %all-to-all-start.5 = ((bf16[8,144,128]{2,1,0:T(8,128)(2,1)}), bf16[8,144,128]{2,1,0:T(8,128)(2,1)S(1)}, u32[]{:S(2)}, u32[]{:S(2)}) async-start(bf16[8,144,128]{2,1,0:T(8,128)(2,1)} %get-tuple-element.69), calls=%async_computation.5 | async-start | bytes 589824 | tf_op jit(solution)/shard_map/all_to_all | solution.py:31
  114.9 1.8 %collective-permute-start.23 = (bf16[8,64,384]{2,1,0:T(8,128)(2,1)S(1)}, bf16[8,64,384]{2,1,0:T(8,128)(2,1)S(1)}, u32[]{:S(2)}, u32[]{:S(2)}) collective-permute-start(bf16[8,64,384]{2,1,0:T(8,128)(2,1)S(1)} %bitcast.17), channel_id=1, source_target_pairs={{0,16},{8,24},{16,0},{24,8},{1,17},{9,25},{17,1},{25,9},{2,18},{10... | collective-permute-start | bytes 1179656 | tf_op jit(solution)/shard_map/ppermute | solution.py:27
  118.3 6.1 %shard_map.205 = (bf16[336,128]{1,0:T(8,128)(2,1)S(1)}, bf16[336,128]{1,0:T(8,128)(2,1)}, bf16[336,128]{1,0:T(8,128)(2,1)}, bf16[336,128]{1,0:T(8,128)(2,1)}) custom-call(bf16[4,480,128]{2,1,0:T(8,128)(2,1)} %all-to-all-done.3.refs_0_, bf16[800,128]{1,0:T(8,128)(2,1)} %get-tuple-element.55.after.refs_1_, bf16[800,128]{1,0:T(8,128)(2,1)S(1)} %copy-done.42, ...), custom_call_target="tpu_custom_call" | custom-call | flops 3355443200 | bytes 1048576 | tf_op jit(solution)/shard_map/pallas_call | solution.py:77
  127.4 2.1 %collective-permute-start.21 = (bf16[336,128]{1,0:T(8,128)(2,1)}, bf16[336,128]{1,0:T(8,128)(2,1)}, u32[]{:S(2)}, u32[]{:S(2)}) collective-permute-start(bf16[336,128]{1,0:T(8,128)(2,1)} %get-tuple-element.67), channel_id=1, source_target_pairs={{0,24},{8,0},{16,8},{24,16},{1,25},{9,1},{17,9},{25,17},{2,26},{10... | collective-permute-start | bytes 258056 | tf_op jit(solution)/shard_map/ppermute | solution.py:27
  129.4 1.6 collective-permute-done.23.l2.o2
  131.0 4.4 %collective-permute-done.24.l3.o3 = bf16[8,64,384]{2,1,0:T(8,128)(2,1)S(1)} collective-permute-done((bf16[8,64,384]{2,1,0:T(8,128)(2,1)S(1)}, bf16[8,64,384]{2,1,0:T(8,128)(2,1)S(1)}, u32[]{:S(2)}, u32[]{:S(2)}) %collective-permute-start.24) | collective-permute-done | bytes 393248 | tf_op jit(solution)/shard_map/ppermute | solution.py:27
  138.3 2.2 %shard_map.208 = (f32[160,2048]{1,0:T(8,128)S(1)}, bf16[160,2048]{1,0:T(8,128)(2,1)S(1)}) custom-call(bf16[336,128]{1,0:T(8,128)(2,1)S(1)} %copy-done.23, bf16[336,128]{1,0:T(8,128)(2,1)} %collective-permute-done.19.p1, bf16[336,128]{1,0:T(8,128)(2,1)} %collective-permute-done.20.p2, bf16[336,128]{1,0:T(8,128)(2,1)} %collective-permute-done.21.p3, ...), custom_call_target="tpu_custom_call" | custom-call | flops 335544320 | bytes 1048576 | tf_op jit(solution)/shard_map/pallas_call | solution.py:77
  140.5 4.2 %collective-permute-start.25 = (bf16[160,2048]{1,0:T(8,128)(2,1)S(1)}, bf16[160,2048]{1,0:T(8,128)(2,1)S(1)}, u32[]{:S(2)}, u32[]{:S(2)}) collective-permute-start(bf16[160,2048]{1,0:T(8,128)(2,1)S(1)} %get-tuple-element.78), channel_id=1, source_target_pairs={{0,4},{4,0},{1,5},{5,1},{2,6},{6,2},{3,7},{7,3},{8,12},{12,8},{9,1... | collective-permute-start | bytes 1966088 | tf_op jit(solution)/shard_map/ppermute | solution.py:27
  144.7 1.7 %collective-permute-done.25 = bf16[160,2048]{1,0:T(8,128)(2,1)S(1)} collective-permute-done((bf16[160,2048]{1,0:T(8,128)(2,1)S(1)}, bf16[160,2048]{1,0:T(8,128)(2,1)S(1)}, u32[]{:S(2)}, u32[]{:S(2)}) %collective-permute-start.25) | collective-permute-done | bytes 655392 | tf_op jit(solution)/shard_map/ppermute | solution.py:27
  147.6 1.9 %collective-permute-start.28 = (bf16[40,2048]{1,0:T(8,128)(2,1)S(1)}, bf16[40,2048]{1,0:T(8,128)(2,1)S(1)}, u32[]{:S(2)}, u32[]{:S(2)}) collective-permute-start(bf16[40,2048]{1,0:T(8,128)(2,1)S(1)} %get-tuple-element.82), channel_id=1, source_target_pairs={{0,3},{1,0},{2,1},{3,2},{4,7},{5,4},{6,5},{7,6},{8,11},{9,8},{10,9... | collective-permute-start | bytes 491528 | tf_op jit(solution)/shard_map/ppermute | solution.py:27
  149.5 7.3 %collective-permute-done.26 = bf16[40,2048]{1,0:T(8,128)(2,1)S(1)} collective-permute-done((bf16[40,2048]{1,0:T(8,128)(2,1)S(1)}, bf16[40,2048]{1,0:T(8,128)(2,1)S(1)}, u32[]{:S(2)}, u32[]{:S(2)}) %collective-permute-start.26) | collective-permute-done | bytes 163872 | tf_op jit(solution)/shard_map/ppermute | solution.py:27
  (158 shorter events, 43.7 us)
Async XLA Ops:
  2.5 20.2 %all-to-all-start = ((bf16[16,48,128]{2,1,0:T(8,128)(2,1)}), bf16[16,48,128]{2,1,0:T(8,128)(2,1)S(1)}, u32[]{:S(2)}, u32[]{:S(2)}) async-start(bf16[16,48,128]{2,1,0:T(8,128)(2,1)} %bitcast.2), calls=%async_computation | async-start | bytes 393216 | tf_op jit(solution)/shard_map/all_to_all | solution.py:31
  22.7 28.0 %all-to-all-start.1 = ((bf16[16,32,512]{2,1,0:T(8,128)(2,1)}), bf16[16,32,512]{2,1,0:T(8,128)(2,1)S(1)}, u32[]{:S(2)}, u32[]{:S(2)}) async-start(bf16[16,32,512]{2,1,0:T(8,128)(2,1)} %bitcast.10), calls=%async_computation.1 | async-start | bytes 1048576 | tf_op jit(solution)/shard_map/all_to_all | solution.py:31
  26.6 14.4 %collective-permute-start = (bf16[160,2048]{1,0:T(8,128)(2,1)S(1)}, bf16[160,2048]{1,0:T(8,128)(2,1)S(1)}, u32[]{:S(2)}, u32[]{:S(2)}) collective-permute-start(bf16[160,2048]{1,0:T(8,128)(2,1)S(1)} %copy-done), channel_id=1, source_target_pairs={{0,4},{4,0},{1,5},{5,1},{2,6},{6,2},{3,7},{7,3},{8,12},{12,8},{9,1... | collective-permute-start | bytes 1966088 | tf_op jit(solution)/shard_map/ppermute | solution.py:27
  28.0 6.5 %collective-permute-start.3 = (bf16[8,96,128]{2,1,0:T(8,128)(2,1)S(1)}, bf16[8,96,128]{2,1,0:T(8,128)(2,1)S(1)}, u32[]{:S(2)}, u32[]{:S(2)}) collective-permute-start(bf16[8,96,128]{2,1,0:T(8,128)(2,1)S(1)} %bitcast.24), channel_id=1, source_target_pairs={{0,24},{8,0},{16,8},{24,16},{1,25},{9,1},{17,9},{25,17},{2,26},{10... | collective-permute-start | bytes 589832 | tf_op jit(solution)/shard_map/ppermute | solution.py:27
  30.8 8.0 %collective-permute-start.1 = (bf16[8,96,128]{2,1,0:T(8,128)(2,1)S(1)}, bf16[8,96,128]{2,1,0:T(8,128)(2,1)S(1)}, u32[]{:S(2)}, u32[]{:S(2)}) collective-permute-start(bf16[8,96,128]{2,1,0:T(8,128)(2,1)S(1)} %bitcast.25), channel_id=1, source_target_pairs={{0,8},{8,16},{16,24},{24,0},{1,9},{9,17},{17,25},{25,1},{2,10},{10... | collective-permute-start | bytes 589832 | tf_op jit(solution)/shard_map/ppermute | solution.py:27
  30.8 10.2 %collective-permute-start.2 = (bf16[8,96,128]{2,1,0:T(8,128)(2,1)S(1)}, bf16[8,96,128]{2,1,0:T(8,128)(2,1)S(1)}, u32[]{:S(2)}, u32[]{:S(2)}) collective-permute-start(bf16[8,96,128]{2,1,0:T(8,128)(2,1)S(1)} %bitcast.26), channel_id=1, source_target_pairs={{0,16},{8,24},{16,0},{24,8},{1,17},{9,25},{17,1},{25,9},{2,18},{10... | collective-permute-start | bytes 589832 | tf_op jit(solution)/shard_map/ppermute | solution.py:27
  45.9 15.3 %collective-permute-start.4 = (bf16[400,128]{1,0:T(8,128)(2,1)S(1)}, bf16[400,128]{1,0:T(8,128)(2,1)S(1)}, u32[]{:S(2)}, u32[]{:S(2)}) collective-permute-start(bf16[400,128]{1,0:T(8,128)(2,1)S(1)} %get-tuple-element.47.refs_0_), channel_id=1, source_target_pairs={{0,1},{1,2},{2,3},{3,0},{4,5},{5,6},{6,7},{7,4},{8,9},{9,10},{10,1... | collective-permute-start | bytes 307208 | tf_op jit(solution)/shard_map/ppermute | solution.py:27
  47.1 14.1 %collective-permute-start.5 = (bf16[400,128]{1,0:T(8,128)(2,1)S(1)}, bf16[400,128]{1,0:T(8,128)(2,1)S(1)}, u32[]{:S(2)}, u32[]{:S(2)}) collective-permute-start(bf16[400,128]{1,0:T(8,128)(2,1)S(1)} %get-tuple-element.47.refs_0_), channel_id=1, source_target_pairs={{0,2},{1,3},{2,0},{3,1},{4,6},{5,7},{6,4},{7,5},{8,10},{9,11},{10,... | collective-permute-start | bytes 307208 | tf_op jit(solution)/shard_map/ppermute | solution.py:27
  49.6 11.7 %collective-permute-start.6 = (bf16[400,128]{1,0:T(8,128)(2,1)S(1)}, bf16[400,128]{1,0:T(8,128)(2,1)S(1)}, u32[]{:S(2)}, u32[]{:S(2)}) collective-permute-start(bf16[400,128]{1,0:T(8,128)(2,1)S(1)} %get-tuple-element.47.refs_0_), channel_id=1, source_target_pairs={{0,3},{1,0},{2,1},{3,2},{4,7},{5,4},{6,5},{7,6},{8,11},{9,8},{10,9... | collective-permute-start | bytes 307208 | tf_op jit(solution)/shard_map/ppermute | solution.py:27
  50.7 26.8 %all-to-all-start.2 = ((bf16[16,32,384]{2,1,0:T(8,128)(2,1)}), bf16[16,32,384]{2,1,0:T(8,128)(2,1)S(1)}, u32[]{:S(2)}, u32[]{:S(2)}) async-start(bf16[16,32,384]{2,1,0:T(8,128)(2,1)} %bitcast.28), calls=%async_computation.2 | async-start | bytes 786432 | tf_op jit(solution)/shard_map/all_to_all | solution.py:31
  62.0 19.8 %collective-permute-start.8 = (bf16[8,64,512]{2,1,0:T(8,128)(2,1)S(1)}, bf16[8,64,512]{2,1,0:T(8,128)(2,1)S(1)}, u32[]{:S(2)}, u32[]{:S(2)}) collective-permute-start(bf16[8,64,512]{2,1,0:T(8,128)(2,1)S(1)} %bitcast.21), channel_id=1, source_target_pairs={{0,8},{8,16},{16,24},{24,0},{1,9},{9,17},{17,25},{25,1},{2,10},{10... | collective-permute-start | bytes 1572872 | tf_op jit(solution)/shard_map/ppermute | solution.py:27
  62.0 21.3 %collective-permute-start.9 = (bf16[8,64,512]{2,1,0:T(8,128)(2,1)S(1)}, bf16[8,64,512]{2,1,0:T(8,128)(2,1)S(1)}, u32[]{:S(2)}, u32[]{:S(2)}) collective-permute-start(bf16[8,64,512]{2,1,0:T(8,128)(2,1)S(1)} %bitcast.22), channel_id=1, source_target_pairs={{0,24},{8,0},{16,8},{24,16},{1,25},{9,1},{17,9},{25,17},{2,26},{10... | collective-permute-start | bytes 1572872 | tf_op jit(solution)/shard_map/ppermute | solution.py:27
  76.2 9.7 %collective-permute-start.12 = (bf16[800,128]{1,0:T(8,128)(2,1)}, bf16[800,128]{1,0:T(8,128)(2,1)S(1)}, u32[]{:S(2)}, u32[]{:S(2)}) collective-permute-start(bf16[800,128]{1,0:T(8,128)(2,1)} %get-tuple-element.55.after.refs_1_), channel_id=1, source_target_pairs={{0,32},{32,64},{64,96},{96,128},{128,160},{160,192},{192,224},{224... | collective-permute-start | bytes 614408 | tf_op jit(solution)/shard_map/ppermute | solution.py:27
  77.6 20.9 %all-to-all-start.3 = ((bf16[4,480,128]{2,1,0:T(8,128)(2,1)}), bf16[4,480,128]{2,1,0:T(8,128)(2,1)}, u32[]{:S(2)}, u32[]{:S(2)}) async-start(bf16[4,480,128]{2,1,0:T(8,128)(2,1)} %copy-done.5), calls=%async_computation.3 | async-start | bytes 983040 | tf_op jit(solution)/shard_map/all_to_all | solution.py:31
  81.8 13.2 %collective-permute-start.10 = (bf16[4,64,512]{2,1,0:T(8,128)(2,1)S(1)}, bf16[4,64,512]{2,1,0:T(8,128)(2,1)S(1)}, u32[]{:S(2)}, u32[]{:S(2)}) collective-permute-start(bf16[4,64,512]{2,1,0:T(8,128)(2,1)S(1)} %slice.27), channel_id=1, source_target_pairs={{0,8},{8,16},{16,24},{24,0},{1,9},{9,17},{17,25},{25,1},{2,10},{10... | collective-permute-start | bytes 786440 | tf_op jit(solution)/shard_map/ppermute | solution.py:27
  83.3 11.7 %collective-permute-start.11 = (bf16[4,64,512]{2,1,0:T(8,128)(2,1)S(1)}, bf16[4,64,512]{2,1,0:T(8,128)(2,1)S(1)}, u32[]{:S(2)}, u32[]{:S(2)}) collective-permute-start(bf16[4,64,512]{2,1,0:T(8,128)(2,1)S(1)} %slice.28), channel_id=1, source_target_pairs={{0,24},{8,0},{16,8},{24,16},{1,25},{9,1},{17,9},{25,17},{2,26},{10... | collective-permute-start | bytes 786440 | tf_op jit(solution)/shard_map/ppermute | solution.py:27
  85.9 6.7 %collective-permute-start.14 = (bf16[800,128]{1,0:T(8,128)(2,1)S(1)}, bf16[800,128]{1,0:T(8,128)(2,1)}, u32[]{:S(2)}, u32[]{:S(2)}) collective-permute-start(bf16[800,128]{1,0:T(8,128)(2,1)S(1)} %collective-permute-done.12.refs_2_), channel_id=1, source_target_pairs={{0,32},{32,64},{64,96},{96,128},{128,160},{160,192},{192,224},{224... | collective-permute-start | bytes 614408 | tf_op jit(solution)/shard_map/ppermute | solution.py:27
  89.8 12.1 %collective-permute-start.15 = (bf16[800,128]{1,0:T(8,128)(2,1)}, bf16[800,128]{1,0:T(8,128)(2,1)}, u32[]{:S(2)}, u32[]{:S(2)}) collective-permute-start(bf16[800,128]{1,0:T(8,128)(2,1)} %collective-permute-done.13.refs_3_), channel_id=1, source_target_pairs={{0,224},{32,0},{64,32},{96,64},{128,96},{160,128},{192,160},{224,1... | collective-permute-start | bytes 614408 | tf_op jit(solution)/shard_map/ppermute | solution.py:27
  92.6 11.0 %collective-permute-start.16 = (bf16[800,128]{1,0:T(8,128)(2,1)}, bf16[800,128]{1,0:T(8,128)(2,1)}, u32[]{:S(2)}, u32[]{:S(2)}) collective-permute-start(bf16[800,128]{1,0:T(8,128)(2,1)} %collective-permute-done.14.refs_4_), channel_id=1, source_target_pairs={{0,32},{32,64},{64,96},{96,128},{128,160},{160,192},{192,224},{224... | collective-permute-start | bytes 614408 | tf_op jit(solution)/shard_map/ppermute | solution.py:27
  98.4 9.0 %all-to-all-start.4 = ((bf16[4,272,128]{2,1,0:T(8,128)(2,1)}), bf16[4,272,128]{2,1,0:T(8,128)(2,1)S(1)}, u32[]{:S(2)}, u32[]{:S(2)}) async-start(bf16[4,272,128]{2,1,0:T(8,128)(2,1)} %get-tuple-element.68), calls=%async_computation.4 | async-start | bytes 557056 | tf_op jit(solution)/shard_map/all_to_all | solution.py:31
  101.9 15.5 %collective-permute-start.17 = (bf16[800,128]{1,0:T(8,128)(2,1)}, bf16[800,128]{1,0:T(8,128)(2,1)}, u32[]{:S(2)}, u32[]{:S(2)}) collective-permute-start(bf16[800,128]{1,0:T(8,128)(2,1)} %collective-permute-done.15.refs_5_), channel_id=1, source_target_pairs={{0,224},{32,0},{64,32},{96,64},{128,96},{160,128},{192,160},{224,1... | collective-permute-start | bytes 614408 | tf_op jit(solution)/shard_map/ppermute | solution.py:27
  103.6 13.8 %collective-permute-start.18 = (bf16[800,128]{1,0:T(8,128)(2,1)}, bf16[800,128]{1,0:T(8,128)(2,1)}, u32[]{:S(2)}, u32[]{:S(2)}) collective-permute-start(bf16[800,128]{1,0:T(8,128)(2,1)} %collective-permute-done.16.refs_6_), channel_id=1, source_target_pairs={{0,32},{32,64},{64,96},{96,128},{128,160},{160,192},{192,224},{224... | collective-permute-start | bytes 614408 | tf_op jit(solution)/shard_map/ppermute | solution.py:27
  109.0 26.4 %all-to-all-start.5 = ((bf16[8,144,128]{2,1,0:T(8,128)(2,1)}), bf16[8,144,128]{2,1,0:T(8,128)(2,1)S(1)}, u32[]{:S(2)}, u32[]{:S(2)}) async-start(bf16[8,144,128]{2,1,0:T(8,128)(2,1)} %get-tuple-element.69), calls=%async_computation.5 | async-start | bytes 589824 | tf_op jit(solution)/shard_map/all_to_all | solution.py:31
  114.5 12.8 %collective-permute-start.22 = (bf16[8,64,384]{2,1,0:T(8,128)(2,1)S(1)}, bf16[8,64,384]{2,1,0:T(8,128)(2,1)S(1)}, u32[]{:S(2)}, u32[]{:S(2)}) collective-permute-start(bf16[8,64,384]{2,1,0:T(8,128)(2,1)S(1)} %bitcast.16), channel_id=1, source_target_pairs={{0,8},{8,16},{16,24},{24,0},{1,9},{9,17},{17,25},{25,1},{2,10},{10... | collective-permute-start | bytes 1179656 | tf_op jit(solution)/shard_map/ppermute | solution.py:27
  114.9 16.1 %collective-permute-start.23 = (bf16[8,64,384]{2,1,0:T(8,128)(2,1)S(1)}, bf16[8,64,384]{2,1,0:T(8,128)(2,1)S(1)}, u32[]{:S(2)}, u32[]{:S(2)}) collective-permute-start(bf16[8,64,384]{2,1,0:T(8,128)(2,1)S(1)} %bitcast.17), channel_id=1, source_target_pairs={{0,16},{8,24},{16,0},{24,8},{1,17},{9,25},{17,1},{25,9},{2,18},{10... | collective-permute-start | bytes 1179656 | tf_op jit(solution)/shard_map/ppermute | solution.py:27
  116.7 18.7 %collective-permute-start.24 = (bf16[8,64,384]{2,1,0:T(8,128)(2,1)S(1)}, bf16[8,64,384]{2,1,0:T(8,128)(2,1)S(1)}, u32[]{:S(2)}, u32[]{:S(2)}) collective-permute-start(bf16[8,64,384]{2,1,0:T(8,128)(2,1)S(1)} %bitcast.18), channel_id=1, source_target_pairs={{0,24},{8,0},{16,8},{24,16},{1,25},{9,1},{17,9},{25,17},{2,26},{10... | collective-permute-start | bytes 1179656 | tf_op jit(solution)/shard_map/ppermute | solution.py:27
  125.1 13.2 %collective-permute-start.19 = (bf16[336,128]{1,0:T(8,128)(2,1)}, bf16[336,128]{1,0:T(8,128)(2,1)}, u32[]{:S(2)}, u32[]{:S(2)}) collective-permute-start(bf16[336,128]{1,0:T(8,128)(2,1)} %get-tuple-element.65), channel_id=1, source_target_pairs={{0,8},{8,16},{16,24},{24,0},{1,9},{9,17},{17,25},{25,1},{2,10},{10... | collective-permute-start | bytes 258056 | tf_op jit(solution)/shard_map/ppermute | solution.py:27
  125.9 12.4 %collective-permute-start.20 = (bf16[336,128]{1,0:T(8,128)(2,1)}, bf16[336,128]{1,0:T(8,128)(2,1)}, u32[]{:S(2)}, u32[]{:S(2)}) collective-permute-start(bf16[336,128]{1,0:T(8,128)(2,1)} %get-tuple-element.66), channel_id=1, source_target_pairs={{0,16},{8,24},{16,0},{24,8},{1,17},{9,25},{17,1},{25,9},{2,18},{10... | collective-permute-start | bytes 258056 | tf_op jit(solution)/shard_map/ppermute | solution.py:27
  127.4 10.9 %collective-permute-start.21 = (bf16[336,128]{1,0:T(8,128)(2,1)}, bf16[336,128]{1,0:T(8,128)(2,1)}, u32[]{:S(2)}, u32[]{:S(2)}) collective-permute-start(bf16[336,128]{1,0:T(8,128)(2,1)} %get-tuple-element.67), channel_id=1, source_target_pairs={{0,24},{8,0},{16,8},{24,16},{1,25},{9,1},{17,9},{25,17},{2,26},{10... | collective-permute-start | bytes 258056 | tf_op jit(solution)/shard_map/ppermute | solution.py:27
  146.7 10.2 %collective-permute-start.26 = (bf16[40,2048]{1,0:T(8,128)(2,1)S(1)}, bf16[40,2048]{1,0:T(8,128)(2,1)S(1)}, u32[]{:S(2)}, u32[]{:S(2)}) collective-permute-start(bf16[40,2048]{1,0:T(8,128)(2,1)S(1)} %get-tuple-element.81), channel_id=1, source_target_pairs={{0,1},{1,2},{2,3},{3,0},{4,5},{5,6},{6,7},{7,4},{8,9},{9,10},{10,1... | collective-permute-start | bytes 491528 | tf_op jit(solution)/shard_map/ppermute | solution.py:27
  147.0 9.8 %collective-permute-start.27 = (bf16[40,2048]{1,0:T(8,128)(2,1)S(1)}, bf16[40,2048]{1,0:T(8,128)(2,1)S(1)}, u32[]{:S(2)}, u32[]{:S(2)}) collective-permute-start(bf16[40,2048]{1,0:T(8,128)(2,1)S(1)} %get-tuple-element.83), channel_id=1, source_target_pairs={{0,2},{1,3},{2,0},{3,1},{4,6},{5,7},{6,4},{7,5},{8,10},{9,11},{10,... | collective-permute-start | bytes 491528 | tf_op jit(solution)/shard_map/ppermute | solution.py:27
  147.6 9.6 %collective-permute-start.28 = (bf16[40,2048]{1,0:T(8,128)(2,1)S(1)}, bf16[40,2048]{1,0:T(8,128)(2,1)S(1)}, u32[]{:S(2)}, u32[]{:S(2)}) collective-permute-start(bf16[40,2048]{1,0:T(8,128)(2,1)S(1)} %get-tuple-element.82), channel_id=1, source_target_pairs={{0,3},{1,0},{2,1},{3,2},{4,7},{5,4},{6,5},{7,6},{8,11},{9,8},{10,9... | collective-permute-start | bytes 491528 | tf_op jit(solution)/shard_map/ppermute | solution.py:27
  (51 other events, 264.8 us)

commit v2 on v1

--- a/solution.py
+++ b/solution.py
@@ -20,6 +20,7 @@
 F32 = jnp.float32
 BF = jnp.bfloat16
 VMEM_GRANT = 20 << 20
+WIDE = ("heads",)
 LOG2E = 1.4426950408889634
 
 
@@ -71,7 +72,7 @@
     return jnp.sum(values * values, axis=-1, keepdims=True)
 
 
-def call(body, outs, args, scratch=(), specs=None, flops=1 << 20, grid=()):
+def call(body, outs, args, name, scratch=(), specs=None, flops=1 << 20, grid=()):
     whole = pl.BlockSpec(memory_space=pltpu.VMEM)
     single = not isinstance(outs, list)
     return pl.pallas_call(
@@ -82,7 +83,9 @@
         out_specs=whole if single else [whole] * len(outs),
         scratch_shapes=list(scratch),
         cost_estimate=pl.CostEstimate(flops=flops, bytes_accessed=1 << 20, transcendentals=0),
-        compiler_params=pltpu.CompilerParams(vmem_limit_bytes=VMEM_GRANT),
+        compiler_params=pltpu.CompilerParams(
+            vmem_limit_bytes=None if name in WIDE else VMEM_GRANT
+        ),
     )(*args)
 
 
@@ -416,6 +419,7 @@
         attend_kernel,
         [made((n + 16, HEAD), BF)] * NY,
         [queries] + list(pieces),
+        "attend",
         scratch=[
             pltpu.VMEM((n, QK), BF),
             pltpu.VMEM((NZ * n, QK), BF),
@@ -494,7 +498,10 @@
         return lax.dynamic_slice_in_dim(weight, c * size, size, 1)
 
     send_b = call(
-        prep_low_kernel, made((NZ, NC, piece * 3 // 2, HEAD), BF), (query_down, latent_down)
+        prep_low_kernel,
+        made((NZ, NC, piece * 3 // 2, HEAD), BF),
+        (query_down, latent_down),
+        "prep_b",
     )
     anywhere = pl.BlockSpec(memory_space=pl.ANY)
     send_a, send_l = call(
@@ -510,6 +517,7 @@
             chain_out.T,
             attend_out.T,
         ),
+        "prep_a",
         specs=[anywhere] + [None] * 7,
     )
 
@@ -544,6 +552,7 @@
             made((1, KVLAT), F32),
         ],
         (query_up, latent_up, query_latent_gain.reshape(8, Q8), latent_gain.reshape(8, KV8)),
+        "ups",
     )
     weights_b[3], early = lax.optimization_barrier((weights_b[3], early))
     cos2, sin2, rates, gain_c, gain_m, wq, wkv, gq, gkv = early
@@ -551,6 +560,7 @@
         low_kernel,
         [made((n, width), BF), made((n * 5 // 4, HEAD), BF), made((n, ROPE), BF)],
         [tokens, other, input_gain[None], rotary_down.T] + weights_b,
+        "low",
         scratch=[
             pltpu.VMEM((NZ, NY, NC * piece * 3 // 2, HEAD), BF),
             pltpu.VMEM((width, HEAD + 32), BF),
@@ -566,6 +576,7 @@
         [made((NY, n * 3 // 2, HEAD), BF), made((n * 5 // 2, HEAD), BF)],
         pieces
         + [swapped, wq, wkv, gq, gkv, rotary, cos2, sin2, query_head_gain[None], key_head_gain[None]],
+        "heads",
         scratch=[pltpu.VMEM((n, QLAT), BF), pltpu.VMEM((n, KVLAT), BF)],
         flops=2 * n * (QLAT * QK + KVLAT * 256),
     )
@@ -582,6 +593,7 @@
             made((NY, 2 * HEAD + 16, HEAD), BF),
         ],
         [kv_piece, rates, normed] + weights_a,
+        "chain",
         scratch=[pltpu.VMEM((NZ, NY, NC * piece, 512), BF), pltpu.SemaphoreType.DMA((5,))],
         specs=[anywhere, None, None] + [anywhere] * 5,
         flops=2 * n * width * 512,
@@ -596,6 +608,7 @@
             made((NZ, HEAD + 16, HEAD), BF),
         ],
         (slab,),
+        "slab",
     )
     outer = exchange(send, "z")
 
@@ -614,6 +627,7 @@
             normed,
             *weights_l,
         ),
+        "close",
         scratch=[pltpu.VMEM((NZ, NY, NC * piece, HEAD), BF), pltpu.SemaphoreType.DMA((4,))],
         specs=[None] * 7 + [anywhere] * 4,
     )
@@ -621,6 +635,7 @@
         final_kernel,
         [made((rows, width), F32), made((rows, width), BF)],
         parts + [chain_mixed, gain_m] + weights_l,
+        "final",
         scratch=[
             pltpu.VMEM((n, 2 * HEAD), F32),
             pltpu.VMEM((NZ, NY, NC * piece, 256), BF),

time: 160 us -> 158 us (0.988)
  local copies, waits for them, and re-layouts: 24.9 us -> 15.5 us
  waiting for transfers between devices: 35.3 us -> 44.6 us
  starting transfers between devices: 74.2 us -> 70 us
  Pallas kernels: 20.6 us -> 22.7 us
    unnamed x96 -> x76, local copies, waits for them, and re-layouts: 24.1 us -> 15.2 us
    all_to_all x6, waiting for transfers between devices: 7.39 us -> 12.3 us  [exchange(): return lax.all_to_all(value, axis, 0, 0, tiled=True)]
    ppermute x29, waiting for transfers between devices: 27.9 us -> 32.3 us  [shift(): lax.ppermute(value, axis, [(i, (i + by) % count) for i in range(count)])]
    all_to_all x6, starting transfers between devices: 37.5 us -> 35.3 us  [exchange(): return lax.all_to_all(value, axis, 0, 0, tiled=True)]
    ppermute x29, starting transfers between devices: 36.7 us -> 34.6 us  [shift(): lax.ppermute(value, axis, [(i, (i + by) % count) for i in range(count)])]
    pallas_call x10, Pallas kernels: 20.6 us -> 22.7 us  [call(): pl.pallas_call(body, out_shape=outs, grid=grid, in_specs=[whole if specs...]
  transfers between devices with their start and end apart: 35 -> 35, of which waited for: 12 -> 13; matrix products, arithmetic and copies ran while one was open for 2% -> 2% of each run, Pallas kernels for 11% -> 13%
where the time goes in v2:
time: 158 us; the launch traced here: 157 us
  starting transfers between devices  70 us (44%)
  waiting for transfers between devices  44.6 us (28%)
  Pallas kernels  22.7 us (14%)
  local copies, waits for them, and re-layouts  15.5 us (10%)
  other arithmetic  3.56 us (2%)
    all_to_all x6, starting transfers between devices, exchange(): return lax.all_to_all(value, axis, 0, 0, tiled=True)  35.3 us
    ppermute x29, starting transfers between devices, shift(): lax.ppermute(value, axis, [(i, (i + by) % count) for i in range(count)])  34.6 us
    ppermute x29, waiting for transfers between devices, shift(): lax.ppermute(value, axis, [(i, (i + by) % count) for i in range(count)])  32.3 us
    pallas_call x10, Pallas kernels, call(): pl.pallas_call(body, out_shape=outs, grid=grid, in_specs=[whole if specs...  22.7 us
    unnamed x76, local copies, waits for them, and re-layouts  15.2 us
    all_to_all x6, waiting for transfers between devices, exchange(): return lax.all_to_all(value, axis, 0, 0, tiled=True)  12.3 us
  transfers between devices with their start and end apart: 35, of which 13 were waited for; matrix products, arithmetic and copies ran while one was open for 2% of the time, Pallas kernels for 13%

profile of v2, /device:TPU:1, one launch (start us, length us, event | category | flops | bytes accessed | tf_op | source)
XLA Modules:
  0.0 156.8 jit_solution(7653593129823364747)
XLA Ops:
  2.5 10.0 %all-to-all-start = ((bf16[16,48,128]{2,1,0:T(8,128)(2,1)}), bf16[16,48,128]{2,1,0:T(8,128)(2,1)S(1)}, u32[]{:S(2)}, u32[]{:S(2)}) async-start(bf16[16,48,128]{2,1,0:T(8,128)(2,1)} %bitcast.2), calls=%async_computation | async-start | bytes 393216 | tf_op jit(solution)/shard_map/all_to_all | solution.py:32
  19.2 3.5 %all-to-all-done = bf16[16,48,128]{2,1,0:T(8,128)(2,1)S(1)} async-done(((bf16[16,48,128]{2,1,0:T(8,128)(2,1)}), bf16[16,48,128]{2,1,0:T(8,128)(2,1)S(1)}, u32[]{:S(2)}, u32[]{:S(2)}) %all-to-all-start) | async-done | bytes 196640 | tf_op jit(solution)/shard_map/all_to_all | solution.py:32
  22.7 3.9 %all-to-all-start.1 = ((bf16[16,32,512]{2,1,0:T(8,128)(2,1)}), bf16[16,32,512]{2,1,0:T(8,128)(2,1)S(1)}, u32[]{:S(2)}, u32[]{:S(2)}) async-start(bf16[16,32,512]{2,1,0:T(8,128)(2,1)} %bitcast.10), calls=%async_computation.1 | async-start | bytes 1048576 | tf_op jit(solution)/shard_map/all_to_all | solution.py:32
  28.0 2.8 %collective-permute-start.3 = (bf16[8,96,128]{2,1,0:T(8,128)(2,1)S(1)}, bf16[8,96,128]{2,1,0:T(8,128)(2,1)S(1)}, u32[]{:S(2)}, u32[]{:S(2)}) collective-permute-start(bf16[8,96,128]{2,1,0:T(8,128)(2,1)S(1)} %bitcast.24), channel_id=1, source_target_pairs={{0,24},{8,0},{16,8},{24,16},{1,25},{9,1},{17,9},{25,17},{2,26},{10... | collective-permute-start | bytes 589832 | tf_op jit(solution)/shard_map/ppermute | solution.py:28
  30.8 1.6 %collective-permute-start.2 = (bf16[8,96,128]{2,1,0:T(8,128)(2,1)S(1)}, bf16[8,96,128]{2,1,0:T(8,128)(2,1)S(1)}, u32[]{:S(2)}, u32[]{:S(2)}) collective-permute-start(bf16[8,96,128]{2,1,0:T(8,128)(2,1)S(1)} %bitcast.26), channel_id=1, source_target_pairs={{0,16},{8,24},{16,0},{24,8},{1,17},{9,25},{17,1},{25,9},{2,18},{10... | collective-permute-start | bytes 589832 | tf_op jit(solution)/shard_map/ppermute | solution.py:28
  34.6 4.3 %collective-permute-done.1.b1 = bf16[8,96,128]{2,1,0:T(8,128)(2,1)S(1)} collective-permute-done((bf16[8,96,128]{2,1,0:T(8,128)(2,1)S(1)}, bf16[8,96,128]{2,1,0:T(8,128)(2,1)S(1)}, u32[]{:S(2)}, u32[]{:S(2)}) %collective-permute-start.1) | collective-permute-done | bytes 196640 | tf_op jit(solution)/shard_map/ppermute | solution.py:28
  38.8 2.2 %collective-permute-done.2.b2 = bf16[8,96,128]{2,1,0:T(8,128)(2,1)S(1)} collective-permute-done((bf16[8,96,128]{2,1,0:T(8,128)(2,1)S(1)}, bf16[8,96,128]{2,1,0:T(8,128)(2,1)S(1)}, u32[]{:S(2)}, u32[]{:S(2)}) %collective-permute-start.2) | collective-permute-done | bytes 196640 | tf_op jit(solution)/shard_map/ppermute | solution.py:28
  42.0 3.9 %shard_map.201 = (bf16[320,2048]{1,0:T(8,128)(2,1)S(1)}, bf16[400,128]{1,0:T(8,128)(2,1)}, bf16[320,64]{1,0:T(8,128)(2,1)S(1)}) custom-call(bf16[160,2048]{1,0:T(8,128)(2,1)S(1)} %copy-done, bf16[160,2048]{1,0:T(8,128)(2,1)S(1)} %collective-permute-done.other, f32[1,2048]{1,0:T(1,128)S(1)} %bitcast.32, bf16[64,2048]{1,0:T(8,128)(2,1)S(1)} %bitcast.29, ...), custom_call_target="tpu_custom_call" | custom-call | flops 419430400 | bytes 1048576 | tf_op jit(solution)/shard_map/pallas_call | solution.py:78
  47.8 2.5 %collective-permute-start.5 = (bf16[400,128]{1,0:T(8,128)(2,1)}, bf16[400,128]{1,0:T(8,128)(2,1)S(1)}, u32[]{:S(2)}, u32[]{:S(2)}) collective-permute-start(bf16[400,128]{1,0:T(8,128)(2,1)} %get-tuple-element.47.refs_0_), channel_id=1, source_target_pairs={{0,2},{1,3},{2,0},{3,1},{4,6},{5,7},{6,4},{7,5},{8,10},{9,11},{10,... | collective-permute-start | bytes 307208 | tf_op jit(solution)/shard_map/ppermute | solution.py:28
  51.4 10.5 %all-to-all-start.2 = ((bf16[16,32,384]{2,1,0:T(8,128)(2,1)}), bf16[16,32,384]{2,1,0:T(8,128)(2,1)S(1)}, u32[]{:S(2)}, u32[]{:S(2)}) async-start(bf16[16,32,384]{2,1,0:T(8,128)(2,1)} %bitcast.28), calls=%async_computation.2 | async-start | bytes 786432 | tf_op jit(solution)/shard_map/all_to_all | solution.py:32
  63.2 2.7 %collective-permute-start.9 = (bf16[8,64,512]{2,1,0:T(8,128)(2,1)S(1)}, bf16[8,64,512]{2,1,0:T(8,128)(2,1)S(1)}, u32[]{:S(2)}, u32[]{:S(2)}) collective-permute-start(bf16[8,64,512]{2,1,0:T(8,128)(2,1)S(1)} %bitcast.22), channel_id=1, source_target_pairs={{0,24},{8,0},{16,8},{24,16},{1,25},{9,1},{17,9},{25,17},{2,26},{10... | collective-permute-start | bytes 1572872 | tf_op jit(solution)/shard_map/ppermute | solution.py:28
  66.7 3.8 %shard_map.202 = (bf16[4,480,128]{2,1,0:T(8,128)(2,1)}, bf16[800,128]{1,0:T(8,128)(2,1)}) custom-call(bf16[400,128]{1,0:T(8,128)(2,1)} %get-tuple-element.47.refs_0_, bf16[400,128]{1,0:T(8,128)(2,1)} %copy-done.30, bf16[400,128]{1,0:T(8,128)(2,1)} %copy-done.31, bf16[400,128]{1,0:T(8,128)(2,1)} %copy-done.32, bf16[1600,128]{1,0:T(8,128)(2,1)} %copy-done.29, ...), custom_call_target="tpu_custom_call" | custom-call | flops 178257920 | bytes 1048576 | tf_op jit(solution)/shard_map/pallas_call | solution.py:78
  70.5 1.8 %collective-permute-start.12 = (bf16[800,128]{1,0:T(8,128)(2,1)}, bf16[800,128]{1,0:T(8,128)(2,1)}, u32[]{:S(2)}, u32[]{:S(2)}) collective-permute-start(bf16[800,128]{1,0:T(8,128)(2,1)} %get-tuple-element.55.after.refs_1_), channel_id=1, source_target_pairs={{0,32},{32,64},{64,96},{96,128},{128,160},{160,192},{192,224},{224... | collective-permute-start | bytes 614408 | tf_op jit(solution)/shard_map/ppermute | solution.py:28
  72.3 4.2 %all-to-all-done.2 = bf16[16,32,384]{2,1,0:T(8,128)(2,1)S(1)} async-done(((bf16[16,32,384]{2,1,0:T(8,128)(2,1)}), bf16[16,32,384]{2,1,0:T(8,128)(2,1)S(1)}, u32[]{:S(2)}, u32[]{:S(2)}) %all-to-all-start.2) | async-done | bytes 393248 | tf_op jit(solution)/shard_map/all_to_all | solution.py:32
  76.4 4.1 %all-to-all-start.3 = ((bf16[4,480,128]{2,1,0:T(8,128)(2,1)}), bf16[4,480,128]{2,1,0:T(8,128)(2,1)}, u32[]{:S(2)}, u32[]{:S(2)}) async-start(bf16[4,480,128]{2,1,0:T(8,128)(2,1)} %get-tuple-element.62), calls=%async_computation.3 | async-start | bytes 983040 | tf_op jit(solution)/shard_map/all_to_all | solution.py:32
  84.9 5.5 %collective-permute-done.13.refs_3_ = bf16[800,128]{1,0:T(8,128)(2,1)} collective-permute-done((bf16[800,128]{1,0:T(8,128)(2,1)S(1)}, bf16[800,128]{1,0:T(8,128)(2,1)}, u32[]{:S(2)}, u32[]{:S(2)}) %collective-permute-start.13) | collective-permute-done | bytes 204832 | tf_op jit(solution)/shard_map/ppermute | solution.py:28
  91.9 3.1 %collective-permute-done.10.a3 = bf16[4,64,512]{2,1,0:T(8,128)(2,1)S(1)} collective-permute-done((bf16[4,64,512]{2,1,0:T(8,128)(2,1)S(1)}, bf16[4,64,512]{2,1,0:T(8,128)(2,1)S(1)}, u32[]{:S(2)}, u32[]{:S(2)}) %collective-permute-start.10) | collective-permute-done | bytes 262176 | tf_op jit(solution)/shard_map/ppermute | solution.py:28
  94.9 2.8 %shard_map.204 = (f32[320,128]{1,0:T(8,128)S(1)}, bf16[2,320,128]{2,1,0:T(8,128)(2,1)S(1)}, bf16[4,272,128]{2,1,0:T(8,128)(2,1)}) custom-call(bf16[800,128]{1,0:T(8,128)(2,1)S(1)} %copy-done.7, f32[2,128]{1,0:T(2,128)S(1)} %dynamic-slice_multiply_fusion.rates, bf16[320,2048]{1,0:T(8,128)(2,1)S(1)} %get-tuple-element.57.normed, ...), custom_call_target="tpu_custom_call" | custom-call | flops 671088640 | bytes 1048576 | tf_op jit(solution)/shard_map/pallas_call | solution.py:78
  99.0 3.5 %all-to-all-start.4 = ((bf16[4,272,128]{2,1,0:T(8,128)(2,1)}), bf16[4,272,128]{2,1,0:T(8,128)(2,1)S(1)}, u32[]{:S(2)}, u32[]{:S(2)}) async-start(bf16[4,272,128]{2,1,0:T(8,128)(2,1)} %get-tuple-element.68), calls=%async_computation.4 | async-start | bytes 557056 | tf_op jit(solution)/shard_map/all_to_all | solution.py:32
  104.1 4.7 %all-to-all-done.4.slab = bf16[4,272,128]{2,1,0:T(8,128)(2,1)S(1)} async-done(((bf16[4,272,128]{2,1,0:T(8,128)(2,1)}), bf16[4,272,128]{2,1,0:T(8,128)(2,1)S(1)}, u32[]{:S(2)}, u32[]{:S(2)}) %all-to-all-start.4) | async-done | bytes 278560 | tf_op jit(solution)/shard_map/all_to_all | solution.py:32
  110.2 3.4 %all-to-all-start.5 = ((bf16[8,144,128]{2,1,0:T(8,128)(2,1)}), bf16[8,144,128]{2,1,0:T(8,128)(2,1)S(1)}, u32[]{:S(2)}, u32[]{:S(2)}) async-start(bf16[8,144,128]{2,1,0:T(8,128)(2,1)} %get-tuple-element.69), calls=%async_computation.5 | async-start | bytes 589824 | tf_op jit(solution)/shard_map/all_to_all | solution.py:32
  114.0 1.8 %collective-permute-start.23 = (bf16[8,64,384]{2,1,0:T(8,128)(2,1)S(1)}, bf16[8,64,384]{2,1,0:T(8,128)(2,1)S(1)}, u32[]{:S(2)}, u32[]{:S(2)}) collective-permute-start(bf16[8,64,384]{2,1,0:T(8,128)(2,1)S(1)} %bitcast.17), channel_id=1, source_target_pairs={{0,16},{8,24},{16,0},{24,8},{1,17},{9,25},{17,1},{25,9},{2,18},{10... | collective-permute-start | bytes 1179656 | tf_op jit(solution)/shard_map/ppermute | solution.py:28
  116.5 6.1 %shard_map.205 = (bf16[336,128]{1,0:T(8,128)(2,1)S(1)}, bf16[336,128]{1,0:T(8,128)(2,1)}, bf16[336,128]{1,0:T(8,128)(2,1)}, bf16[336,128]{1,0:T(8,128)(2,1)}) custom-call(bf16[4,480,128]{2,1,0:T(8,128)(2,1)} %all-to-all-done.3.refs_0_, bf16[800,128]{1,0:T(8,128)(2,1)S(1)} %copy-done.7, bf16[800,128]{1,0:T(8,128)(2,1)} %collective-permute-done.12.refs_2_, ...), custom_call_target="tpu_custom_call" | custom-call | flops 3355443200 | bytes 1048576 | tf_op jit(solution)/shard_map/pallas_call | solution.py:78
  124.0 1.5 collective-permute-start.20
  125.5 2.1 %collective-permute-start.21 = (bf16[336,128]{1,0:T(8,128)(2,1)}, bf16[336,128]{1,0:T(8,128)(2,1)}, u32[]{:S(2)}, u32[]{:S(2)}) collective-permute-start(bf16[336,128]{1,0:T(8,128)(2,1)} %get-tuple-element.67), channel_id=1, source_target_pairs={{0,24},{8,0},{16,8},{24,16},{1,25},{9,1},{17,9},{25,17},{2,26},{10... | collective-permute-start | bytes 258056 | tf_op jit(solution)/shard_map/ppermute | solution.py:28
  127.6 4.3 %collective-permute-done.23.l2.o2 = bf16[8,64,384]{2,1,0:T(8,128)(2,1)S(1)} collective-permute-done((bf16[8,64,384]{2,1,0:T(8,128)(2,1)S(1)}, bf16[8,64,384]{2,1,0:T(8,128)(2,1)S(1)}, u32[]{:S(2)}, u32[]{:S(2)}) %collective-permute-start.23) | collective-permute-done | bytes 393248 | tf_op jit(solution)/shard_map/ppermute | solution.py:28
  131.9 2.4 %collective-permute-done.24.l3.o3 = bf16[8,64,384]{2,1,0:T(8,128)(2,1)S(1)} collective-permute-done((bf16[8,64,384]{2,1,0:T(8,128)(2,1)S(1)}, bf16[8,64,384]{2,1,0:T(8,128)(2,1)S(1)}, u32[]{:S(2)}, u32[]{:S(2)}) %collective-permute-start.24) | collective-permute-done | bytes 393248 | tf_op jit(solution)/shard_map/ppermute | solution.py:28
  138.2 2.1 %shard_map.208 = (f32[160,2048]{1,0:T(8,128)S(1)}, bf16[160,2048]{1,0:T(8,128)(2,1)S(1)}) custom-call(bf16[336,128]{1,0:T(8,128)(2,1)S(1)} %copy-done.15, bf16[336,128]{1,0:T(8,128)(2,1)S(1)} %collective-permute-done.19.p1, bf16[336,128]{1,0:T(8,128)(2,1)S(1)} %collective-permute-done.20.p2, bf16[336,128]{1,0:T(8,128)(2,1)} %collective-permute-done.21.p3, ...), custom_call_target="tpu_custom_call" | custom-call | flops 335544320 | bytes 1048576 | tf_op jit(solution)/shard_map/pallas_call | solution.py:78
  140.3 3.1 %collective-permute-start.25 = (bf16[160,2048]{1,0:T(8,128)(2,1)S(1)}, bf16[160,2048]{1,0:T(8,128)(2,1)S(1)}, u32[]{:S(2)}, u32[]{:S(2)}) collective-permute-start(bf16[160,2048]{1,0:T(8,128)(2,1)S(1)} %get-tuple-element.78), channel_id=1, source_target_pairs={{0,4},{4,0},{1,5},{5,1},{2,6},{6,2},{3,7},{7,3},{8,12},{12,8},{9,1... | collective-permute-start | bytes 1966088 | tf_op jit(solution)/shard_map/ppermute | solution.py:28
  143.4 1.7 %collective-permute-done.25 = bf16[160,2048]{1,0:T(8,128)(2,1)S(1)} collective-permute-done((bf16[160,2048]{1,0:T(8,128)(2,1)S(1)}, bf16[160,2048]{1,0:T(8,128)(2,1)S(1)}, u32[]{:S(2)}, u32[]{:S(2)}) %collective-permute-start.25) | collective-permute-done | bytes 655392 | tf_op jit(solution)/shard_map/ppermute | solution.py:28
  146.4 1.9 %collective-permute-start.28 = (bf16[40,2048]{1,0:T(8,128)(2,1)S(1)}, bf16[40,2048]{1,0:T(8,128)(2,1)S(1)}, u32[]{:S(2)}, u32[]{:S(2)}) collective-permute-start(bf16[40,2048]{1,0:T(8,128)(2,1)S(1)} %get-tuple-element.82), channel_id=1, source_target_pairs={{0,3},{1,0},{2,1},{3,2},{4,7},{5,4},{6,5},{7,6},{8,11},{9,8},{10,9... | collective-permute-start | bytes 491528 | tf_op jit(solution)/shard_map/ppermute | solution.py:28
  148.3 7.3 %collective-permute-done.26 = bf16[40,2048]{1,0:T(8,128)(2,1)S(1)} collective-permute-done((bf16[40,2048]{1,0:T(8,128)(2,1)S(1)}, bf16[40,2048]{1,0:T(8,128)(2,1)S(1)}, u32[]{:S(2)}, u32[]{:S(2)}) %collective-permute-start.26) | collective-permute-done | bytes 163872 | tf_op jit(solution)/shard_map/ppermute | solution.py:28
  (138 shorter events, 37.4 us)
Async XLA Ops:
  2.5 20.2 %all-to-all-start = ((bf16[16,48,128]{2,1,0:T(8,128)(2,1)}), bf16[16,48,128]{2,1,0:T(8,128)(2,1)S(1)}, u32[]{:S(2)}, u32[]{:S(2)}) async-start(bf16[16,48,128]{2,1,0:T(8,128)(2,1)} %bitcast.2), calls=%async_computation | async-start | bytes 393216 | tf_op jit(solution)/shard_map/all_to_all | solution.py:32
  22.7 28.7 %all-to-all-start.1 = ((bf16[16,32,512]{2,1,0:T(8,128)(2,1)}), bf16[16,32,512]{2,1,0:T(8,128)(2,1)S(1)}, u32[]{:S(2)}, u32[]{:S(2)}) async-start(bf16[16,32,512]{2,1,0:T(8,128)(2,1)} %bitcast.10), calls=%async_computation.1 | async-start | bytes 1048576 | tf_op jit(solution)/shard_map/all_to_all | solution.py:32
  26.6 14.4 %collective-permute-start = (bf16[160,2048]{1,0:T(8,128)(2,1)S(1)}, bf16[160,2048]{1,0:T(8,128)(2,1)S(1)}, u32[]{:S(2)}, u32[]{:S(2)}) collective-permute-start(bf16[160,2048]{1,0:T(8,128)(2,1)S(1)} %copy-done), channel_id=1, source_target_pairs={{0,4},{4,0},{1,5},{5,1},{2,6},{6,2},{3,7},{7,3},{8,12},{12,8},{9,1... | collective-permute-start | bytes 1966088 | tf_op jit(solution)/shard_map/ppermute | solution.py:28
  30.8 8.0 %collective-permute-start.1 = (bf16[8,96,128]{2,1,0:T(8,128)(2,1)S(1)}, bf16[8,96,128]{2,1,0:T(8,128)(2,1)S(1)}, u32[]{:S(2)}, u32[]{:S(2)}) collective-permute-start(bf16[8,96,128]{2,1,0:T(8,128)(2,1)S(1)} %bitcast.25), channel_id=1, source_target_pairs={{0,8},{8,16},{16,24},{24,0},{1,9},{9,17},{17,25},{25,1},{2,10},{10... | collective-permute-start | bytes 589832 | tf_op jit(solution)/shard_map/ppermute | solution.py:28
  30.8 10.2 %collective-permute-start.2 = (bf16[8,96,128]{2,1,0:T(8,128)(2,1)S(1)}, bf16[8,96,128]{2,1,0:T(8,128)(2,1)S(1)}, u32[]{:S(2)}, u32[]{:S(2)}) collective-permute-start(bf16[8,96,128]{2,1,0:T(8,128)(2,1)S(1)} %bitcast.26), channel_id=1, source_target_pairs={{0,16},{8,24},{16,0},{24,8},{1,17},{9,25},{17,1},{25,9},{2,18},{10... | collective-permute-start | bytes 589832 | tf_op jit(solution)/shard_map/ppermute | solution.py:28
  46.6 15.3 %collective-permute-start.4 = (bf16[400,128]{1,0:T(8,128)(2,1)}, bf16[400,128]{1,0:T(8,128)(2,1)S(1)}, u32[]{:S(2)}, u32[]{:S(2)}) collective-permute-start(bf16[400,128]{1,0:T(8,128)(2,1)} %get-tuple-element.47.refs_0_), channel_id=1, source_target_pairs={{0,1},{1,2},{2,3},{3,0},{4,5},{5,6},{6,7},{7,4},{8,9},{9,10},{10,1... | collective-permute-start | bytes 307208 | tf_op jit(solution)/shard_map/ppermute | solution.py:28
  47.8 14.1 %collective-permute-start.5 = (bf16[400,128]{1,0:T(8,128)(2,1)}, bf16[400,128]{1,0:T(8,128)(2,1)S(1)}, u32[]{:S(2)}, u32[]{:S(2)}) collective-permute-start(bf16[400,128]{1,0:T(8,128)(2,1)} %get-tuple-element.47.refs_0_), channel_id=1, source_target_pairs={{0,2},{1,3},{2,0},{3,1},{4,6},{5,7},{6,4},{7,5},{8,10},{9,11},{10,... | collective-permute-start | bytes 307208 | tf_op jit(solution)/shard_map/ppermute | solution.py:28
  50.3 11.7 %collective-permute-start.6 = (bf16[400,128]{1,0:T(8,128)(2,1)}, bf16[400,128]{1,0:T(8,128)(2,1)S(1)}, u32[]{:S(2)}, u32[]{:S(2)}) collective-permute-start(bf16[400,128]{1,0:T(8,128)(2,1)} %get-tuple-element.47.refs_0_), channel_id=1, source_target_pairs={{0,3},{1,0},{2,1},{3,2},{4,7},{5,4},{6,5},{7,6},{8,11},{9,8},{10,9... | collective-permute-start | bytes 307208 | tf_op jit(solution)/shard_map/ppermute | solution.py:28
  51.4 25.0 %all-to-all-start.2 = ((bf16[16,32,384]{2,1,0:T(8,128)(2,1)}), bf16[16,32,384]{2,1,0:T(8,128)(2,1)S(1)}, u32[]{:S(2)}, u32[]{:S(2)}) async-start(bf16[16,32,384]{2,1,0:T(8,128)(2,1)} %bitcast.28), calls=%async_computation.2 | async-start | bytes 786432 | tf_op jit(solution)/shard_map/all_to_all | solution.py:32
  63.2 17.4 %collective-permute-start.8 = (bf16[8,64,512]{2,1,0:T(8,128)(2,1)S(1)}, bf16[8,64,512]{2,1,0:T(8,128)(2,1)S(1)}, u32[]{:S(2)}, u32[]{:S(2)}) collective-permute-start(bf16[8,64,512]{2,1,0:T(8,128)(2,1)S(1)} %bitcast.21), channel_id=1, source_target_pairs={{0,8},{8,16},{16,24},{24,0},{1,9},{9,17},{17,25},{25,1},{2,10},{10... | collective-permute-start | bytes 1572872 | tf_op jit(solution)/shard_map/ppermute | solution.py:28
  63.2 18.9 %collective-permute-start.9 = (bf16[8,64,512]{2,1,0:T(8,128)(2,1)S(1)}, bf16[8,64,512]{2,1,0:T(8,128)(2,1)S(1)}, u32[]{:S(2)}, u32[]{:S(2)}) collective-permute-start(bf16[8,64,512]{2,1,0:T(8,128)(2,1)S(1)} %bitcast.22), channel_id=1, source_target_pairs={{0,24},{8,0},{16,8},{24,16},{1,25},{9,1},{17,9},{25,17},{2,26},{10... | collective-permute-start | bytes 1572872 | tf_op jit(solution)/shard_map/ppermute | solution.py:28
  70.5 13.0 %collective-permute-start.12 = (bf16[800,128]{1,0:T(8,128)(2,1)}, bf16[800,128]{1,0:T(8,128)(2,1)}, u32[]{:S(2)}, u32[]{:S(2)}) collective-permute-start(bf16[800,128]{1,0:T(8,128)(2,1)} %get-tuple-element.55.after.refs_1_), channel_id=1, source_target_pairs={{0,32},{32,64},{64,96},{96,128},{128,160},{160,192},{192,224},{224... | collective-permute-start | bytes 614408 | tf_op jit(solution)/shard_map/ppermute | solution.py:28
  76.4 22.6 %all-to-all-start.3 = ((bf16[4,480,128]{2,1,0:T(8,128)(2,1)}), bf16[4,480,128]{2,1,0:T(8,128)(2,1)}, u32[]{:S(2)}, u32[]{:S(2)}) async-start(bf16[4,480,128]{2,1,0:T(8,128)(2,1)} %get-tuple-element.62), calls=%async_computation.3 | async-start | bytes 983040 | tf_op jit(solution)/shard_map/all_to_all | solution.py:32
  80.6 14.3 %collective-permute-start.10 = (bf16[4,64,512]{2,1,0:T(8,128)(2,1)S(1)}, bf16[4,64,512]{2,1,0:T(8,128)(2,1)S(1)}, u32[]{:S(2)}, u32[]{:S(2)}) collective-permute-start(bf16[4,64,512]{2,1,0:T(8,128)(2,1)S(1)} %slice.27), channel_id=1, source_target_pairs={{0,8},{8,16},{16,24},{24,0},{1,9},{9,17},{17,25},{25,1},{2,10},{10... | collective-permute-start | bytes 786440 | tf_op jit(solution)/shard_map/ppermute | solution.py:28
  82.1 12.8 %collective-permute-start.11 = (bf16[4,64,512]{2,1,0:T(8,128)(2,1)S(1)}, bf16[4,64,512]{2,1,0:T(8,128)(2,1)S(1)}, u32[]{:S(2)}, u32[]{:S(2)}) collective-permute-start(bf16[4,64,512]{2,1,0:T(8,128)(2,1)S(1)} %slice.28), channel_id=1, source_target_pairs={{0,24},{8,0},{16,8},{24,16},{1,25},{9,1},{17,9},{25,17},{2,26},{10... | collective-permute-start | bytes 786440 | tf_op jit(solution)/shard_map/ppermute | solution.py:28
  83.5 6.9 %collective-permute-start.13 = (bf16[800,128]{1,0:T(8,128)(2,1)S(1)}, bf16[800,128]{1,0:T(8,128)(2,1)}, u32[]{:S(2)}, u32[]{:S(2)}) collective-permute-start(bf16[800,128]{1,0:T(8,128)(2,1)S(1)} %copy-done.7), channel_id=1, source_target_pairs={{0,224},{32,0},{64,32},{96,64},{128,96},{160,128},{192,160},{224,1... | collective-permute-start | bytes 614408 | tf_op jit(solution)/shard_map/ppermute | solution.py:28
  83.5 6.9 %collective-permute-start.14 = (bf16[800,128]{1,0:T(8,128)(2,1)}, bf16[800,128]{1,0:T(8,128)(2,1)}, u32[]{:S(2)}, u32[]{:S(2)}) collective-permute-start(bf16[800,128]{1,0:T(8,128)(2,1)} %collective-permute-done.12.refs_2_), channel_id=1, source_target_pairs={{0,32},{32,64},{64,96},{96,128},{128,160},{160,192},{192,224},{224... | collective-permute-start | bytes 614408 | tf_op jit(solution)/shard_map/ppermute | solution.py:28
  90.4 12.1 %collective-permute-start.15 = (bf16[800,128]{1,0:T(8,128)(2,1)}, bf16[800,128]{1,0:T(8,128)(2,1)}, u32[]{:S(2)}, u32[]{:S(2)}) collective-permute-start(bf16[800,128]{1,0:T(8,128)(2,1)} %collective-permute-done.13.refs_3_), channel_id=1, source_target_pairs={{0,224},{32,0},{64,32},{96,64},{128,96},{160,128},{192,160},{224,1... | collective-permute-start | bytes 614408 | tf_op jit(solution)/shard_map/ppermute | solution.py:28
  90.4 12.2 %collective-permute-start.16 = (bf16[800,128]{1,0:T(8,128)(2,1)}, bf16[800,128]{1,0:T(8,128)(2,1)}, u32[]{:S(2)}, u32[]{:S(2)}) collective-permute-start(bf16[800,128]{1,0:T(8,128)(2,1)} %collective-permute-done.14.refs_4_), channel_id=1, source_target_pairs={{0,32},{32,64},{64,96},{96,128},{128,160},{160,192},{192,224},{224... | collective-permute-start | bytes 614408 | tf_op jit(solution)/shard_map/ppermute | solution.py:28
  99.0 9.7 %all-to-all-start.4 = ((bf16[4,272,128]{2,1,0:T(8,128)(2,1)}), bf16[4,272,128]{2,1,0:T(8,128)(2,1)S(1)}, u32[]{:S(2)}, u32[]{:S(2)}) async-start(bf16[4,272,128]{2,1,0:T(8,128)(2,1)} %get-tuple-element.68), calls=%async_computation.4 | async-start | bytes 557056 | tf_op jit(solution)/shard_map/all_to_all | solution.py:32
  102.5 14.0 %collective-permute-start.17 = (bf16[800,128]{1,0:T(8,128)(2,1)}, bf16[800,128]{1,0:T(8,128)(2,1)}, u32[]{:S(2)}, u32[]{:S(2)}) collective-permute-start(bf16[800,128]{1,0:T(8,128)(2,1)} %collective-permute-done.15.refs_5_), channel_id=1, source_target_pairs={{0,224},{32,0},{64,32},{96,64},{128,96},{160,128},{192,160},{224,1... | collective-permute-start | bytes 614408 | tf_op jit(solution)/shard_map/ppermute | solution.py:28
  102.6 13.9 %collective-permute-start.18 = (bf16[800,128]{1,0:T(8,128)(2,1)}, bf16[800,128]{1,0:T(8,128)(2,1)}, u32[]{:S(2)}, u32[]{:S(2)}) collective-permute-start(bf16[800,128]{1,0:T(8,128)(2,1)} %collective-permute-done.16.refs_6_), channel_id=1, source_target_pairs={{0,32},{32,64},{64,96},{96,128},{128,160},{160,192},{192,224},{224... | collective-permute-start | bytes 614408 | tf_op jit(solution)/shard_map/ppermute | solution.py:28
  110.2 24.1 %all-to-all-start.5 = ((bf16[8,144,128]{2,1,0:T(8,128)(2,1)}), bf16[8,144,128]{2,1,0:T(8,128)(2,1)S(1)}, u32[]{:S(2)}, u32[]{:S(2)}) async-start(bf16[8,144,128]{2,1,0:T(8,128)(2,1)} %get-tuple-element.69), calls=%async_computation.5 | async-start | bytes 589824 | tf_op jit(solution)/shard_map/all_to_all | solution.py:32
  113.6 11.9 %collective-permute-start.22 = (bf16[8,64,384]{2,1,0:T(8,128)(2,1)S(1)}, bf16[8,64,384]{2,1,0:T(8,128)(2,1)S(1)}, u32[]{:S(2)}, u32[]{:S(2)}) collective-permute-start(bf16[8,64,384]{2,1,0:T(8,128)(2,1)S(1)} %bitcast.16), channel_id=1, source_target_pairs={{0,8},{8,16},{16,24},{24,0},{1,9},{9,17},{17,25},{25,1},{2,10},{10... | collective-permute-start | bytes 1179656 | tf_op jit(solution)/shard_map/ppermute | solution.py:28
  114.0 17.9 %collective-permute-start.23 = (bf16[8,64,384]{2,1,0:T(8,128)(2,1)S(1)}, bf16[8,64,384]{2,1,0:T(8,128)(2,1)S(1)}, u32[]{:S(2)}, u32[]{:S(2)}) collective-permute-start(bf16[8,64,384]{2,1,0:T(8,128)(2,1)S(1)} %bitcast.17), channel_id=1, source_target_pairs={{0,16},{8,24},{16,0},{24,8},{1,17},{9,25},{17,1},{25,9},{2,18},{10... | collective-permute-start | bytes 1179656 | tf_op jit(solution)/shard_map/ppermute | solution.py:28
  115.8 18.6 %collective-permute-start.24 = (bf16[8,64,384]{2,1,0:T(8,128)(2,1)S(1)}, bf16[8,64,384]{2,1,0:T(8,128)(2,1)S(1)}, u32[]{:S(2)}, u32[]{:S(2)}) collective-permute-start(bf16[8,64,384]{2,1,0:T(8,128)(2,1)S(1)} %bitcast.18), channel_id=1, source_target_pairs={{0,24},{8,0},{16,8},{24,16},{1,25},{9,1},{17,9},{25,17},{2,26},{10... | collective-permute-start | bytes 1179656 | tf_op jit(solution)/shard_map/ppermute | solution.py:28
  123.3 14.9 %collective-permute-start.19 = (bf16[336,128]{1,0:T(8,128)(2,1)}, bf16[336,128]{1,0:T(8,128)(2,1)S(1)}, u32[]{:S(2)}, u32[]{:S(2)}) collective-permute-start(bf16[336,128]{1,0:T(8,128)(2,1)} %get-tuple-element.65), channel_id=1, source_target_pairs={{0,8},{8,16},{16,24},{24,0},{1,9},{9,17},{17,25},{25,1},{2,10},{10... | collective-permute-start | bytes 258056 | tf_op jit(solution)/shard_map/ppermute | solution.py:28
  124.0 14.1 %collective-permute-start.20 = (bf16[336,128]{1,0:T(8,128)(2,1)}, bf16[336,128]{1,0:T(8,128)(2,1)S(1)}, u32[]{:S(2)}, u32[]{:S(2)}) collective-permute-start(bf16[336,128]{1,0:T(8,128)(2,1)} %get-tuple-element.66), channel_id=1, source_target_pairs={{0,16},{8,24},{16,0},{24,8},{1,17},{9,25},{17,1},{25,9},{2,18},{10... | collective-permute-start | bytes 258056 | tf_op jit(solution)/shard_map/ppermute | solution.py:28
  125.5 12.6 %collective-permute-start.21 = (bf16[336,128]{1,0:T(8,128)(2,1)}, bf16[336,128]{1,0:T(8,128)(2,1)}, u32[]{:S(2)}, u32[]{:S(2)}) collective-permute-start(bf16[336,128]{1,0:T(8,128)(2,1)} %get-tuple-element.67), channel_id=1, source_target_pairs={{0,24},{8,0},{16,8},{24,16},{1,25},{9,1},{17,9},{25,17},{2,26},{10... | collective-permute-start | bytes 258056 | tf_op jit(solution)/shard_map/ppermute | solution.py:28
  145.4 10.2 %collective-permute-start.26 = (bf16[40,2048]{1,0:T(8,128)(2,1)S(1)}, bf16[40,2048]{1,0:T(8,128)(2,1)S(1)}, u32[]{:S(2)}, u32[]{:S(2)}) collective-permute-start(bf16[40,2048]{1,0:T(8,128)(2,1)S(1)} %get-tuple-element.81), channel_id=1, source_target_pairs={{0,1},{1,2},{2,3},{3,0},{4,5},{5,6},{6,7},{7,4},{8,9},{9,10},{10,1... | collective-permute-start | bytes 491528 | tf_op jit(solution)/shard_map/ppermute | solution.py:28
  145.8 9.8 %collective-permute-start.27 = (bf16[40,2048]{1,0:T(8,128)(2,1)S(1)}, bf16[40,2048]{1,0:T(8,128)(2,1)S(1)}, u32[]{:S(2)}, u32[]{:S(2)}) collective-permute-start(bf16[40,2048]{1,0:T(8,128)(2,1)S(1)} %get-tuple-element.83), channel_id=1, source_target_pairs={{0,2},{1,3},{2,0},{3,1},{4,6},{5,7},{6,4},{7,5},{8,10},{9,11},{10,... | collective-permute-start | bytes 491528 | tf_op jit(solution)/shard_map/ppermute | solution.py:28
  146.4 9.6 %collective-permute-start.28 = (bf16[40,2048]{1,0:T(8,128)(2,1)S(1)}, bf16[40,2048]{1,0:T(8,128)(2,1)S(1)}, u32[]{:S(2)}, u32[]{:S(2)}) collective-permute-start(bf16[40,2048]{1,0:T(8,128)(2,1)S(1)} %get-tuple-element.82), channel_id=1, source_target_pairs={{0,3},{1,0},{2,1},{3,2},{4,7},{5,4},{6,5},{7,6},{8,11},{9,8},{10,9... | collective-permute-start | bytes 491528 | tf_op jit(solution)/shard_map/ppermute | solution.py:28
  (41 other events, 252.1 us)
